TPU v7x, 256 devices: a 2x2x32 block of a 4x8x32 slice. The times are simulated.
256 devices in a mesh: grp: 4 (over y, x), ep: 64 (over z, core).
Axes of the slice: x: 2, y: 2, z: 32, core: 2. Of those that a mesh axis runs over, the one named last changes fastest.
The devices are a block of a 4x8x32 slice.
Arguments:
- tokens: bfloat16 [2048, 2048], P(('grp', 'ep')), parts along dimension 0, may hold values from -6 to 6
- first_gain: bfloat16 [2048], replicated, may hold values from 0.099609375 to 1.8984375
- query_weight: bfloat16 [2048, 1024], P(None, 'ep'), may hold values from -0.125 to 0.125
- key_weight: bfloat16 [2048, 1024], P(None, 'ep'), may hold values from -0.125 to 0.125
- value_weight: bfloat16 [2048, 1024], P(None, 'ep'), may hold values from -0.125 to 0.125
- outgate_weight: bfloat16 [2048, 1024], P(None, 'ep'), may hold values from -0.125 to 0.125
- igate_weight: bfloat16 [2048, 8], replicated, may hold values from -0.125 to 0.125
- fgate_weight: bfloat16 [2048, 8], replicated, may hold values from -0.125 to 0.125
- igate_bias: float32 [8], replicated, may hold values from -2 to 1
- fgate_bias: float32 [8], replicated, may hold values from -1 to 4
- memory_state: float32 [2048, 8, 128, 128], P(('grp', 'ep')), parts along dimension 0, may hold values from -0.6 to 0.6
- norm_state: float32 [2048, 8, 128], P(('grp', 'ep')), parts along dimension 0, may hold values from -0.6 to 0.6
- max_state: float32 [2048, 8], P(('grp', 'ep')), parts along dimension 0, may hold values from -1 to 2
- head_gain: bfloat16 [1024], replicated, may hold values from 0.099609375 to 1.8984375
- out_weight: bfloat16 [1024, 2048], P('ep'), may hold values from -0.1875 to 0.1875
- second_gain: bfloat16 [2048], replicated, may hold values from 0.099609375 to 1.8984375
- expert_ids: int32 [2048, 6], P(('grp', 'ep')), parts along dimension 0, may hold values from 0 to 63, all different within a row; in each aligned block of 8 rows (0 to 7, 8 to 15, ...) at most 2 rows name the same one
- route_weight: float32 [2048, 6], P(('grp', 'ep')), parts along dimension 0, may hold values from 0.2 to 1
- expert_gate: bfloat16 [64, 2048, 256], P('ep'), may hold values from -0.125 to 0.125
- expert_up: bfloat16 [64, 2048, 256], P('ep'), may hold values from -0.125 to 0.125
- expert_down: bfloat16 [64, 256, 2048], P('ep'), may hold values from -0.375 to 0.375
- shared_gate: bfloat16 [2048, 256], P('ep'), may hold values from -0.125 to 0.125
- shared_up: bfloat16 [2048, 256], P('ep'), may hold values from -0.125 to 0.125
- shared_down: bfloat16 [256, 2048], P(None, 'ep'), may hold values from -0.375 to 0.375
Outputs:
- mixed_out: bfloat16 [2048, 2048], P(('grp', 'ep')), parts along dimension 0
- memory_next: float32 [2048, 8, 128, 128], P(('grp', 'ep')), parts along dimension 0
- norm_next: float32 [2048, 8, 128], P(('grp', 'ep')), parts along dimension 0
- max_next: float32 [2048, 8], P(('grp', 'ep')), parts along dimension 0
There are 4 independent parts, one for each index of `grp`. A program takes and returns all parts, laid end to end along the dimension named above; an argument that names none is the same for every part. Nothing has to cross between parts.
Inputs may be any that keep to these rules, and one draw needn't show every extreme that they name: `expert_ids`: each row names 6 different experts. Among the rows of one device no expert is named by more than 2 rows, and in every draw some expert is named by exactly 2 rows of some device.
All inputs are finite; a program needn't handle non-finite values.
Results may differ from a plain program's by a relative error of at most 0.013.
Values may be sent and summed in bfloat16 or wider, within the bound.
No kernel may reach another device: no remote copies, remote signals or barrier semaphores. Data moves between devices by JAX's collectives and lax.ppermute only.
A program may use at most 64 MiB of HBM per device.

v0:
```python
import jax
import jax.numpy as jnp
from jax import lax
from jax.sharding import Mesh
from jax.sharding import PartitionSpec as P

EP = ("ep_0", "ep_1")
GRP_EP = ("grp", "ep_0", "ep_1")


epsilon = 1e-06


def laid_out(parts, dim):
    parts = jnp.moveaxis(parts, 0, dim)
    lengths = parts.shape
    return parts.reshape(*lengths[:dim], lengths[dim] * lengths[dim + 1], *lengths[dim + 2 :])


def stacked_from(x, axes, order):
    parts = x[None]
    for k in order:
        parts = lax.all_gather(parts, axes[k], axis=0, tiled=True)
    current = [lax.axis_size(axes[k]) for k in reversed(order)]
    parts = parts.reshape(*current, *x.shape)
    turned = sorted(range(len(order)), key=lambda place: order[len(order) - 1 - place])
    return parts.transpose(*turned, *range(len(order), parts.ndim)).reshape(-1, *x.shape)


def gather_axes(x, axes, order, dim):
    return laid_out(stacked_from(x, axes, order), dim)


def side_by_side(arrays, axis, dim, along):
    both = jnp.concatenate(arrays, axis=along)
    whole, at, outs = (lax.all_gather(both, axis, axis=dim, tiled=True), 0, [])
    for a in arrays:
        outs.append(lax.slice_in_dim(whole, at, at + a.shape[along], axis=along))
        at += a.shape[along]
    return tuple(outs)


def rms_scale(values, gain):
    return (
        values
        * lax.rsqrt(jnp.mean(values * values, axis=-1, keepdims=True) + epsilon)
        * gain.astype(jnp.float32)
    )


def cell_step(
    normed,
    query,
    key_proj,
    value_proj,
    outgate,
    igate_weight,
    fgate_weight,
    igate_bias,
    fgate_bias,
    memory_state,
    norm_state,
    max_state,
    head_gain,
):
    row_count, head_count = max_state.shape
    head_size = memory_state.shape[-1]
    input_gate = jnp.dot(normed, igate_weight, preferred_element_type=jnp.float32) + igate_bias
    forget_log = jax.nn.log_sigmoid(
        jnp.dot(normed, fgate_weight, preferred_element_type=jnp.float32) + fgate_bias
    )
    query_heads = query.astype(jnp.float32).reshape(row_count, head_count, head_size)
    key_heads = key_proj.astype(jnp.float32).reshape(
        row_count, head_count, head_size
    ) * head_size ** (-0.5)
    value_heads = value_proj.astype(jnp.float32).reshape(row_count, head_count, head_size)
    max_next = jnp.maximum(forget_log + max_state, input_gate)
    decay_rate = jnp.exp(forget_log + max_state - max_next)
    injected = jnp.exp(input_gate - max_next)
    memory_next = decay_rate[:, :, None, None] * memory_state + injected[:, :, None, None] * (
        key_heads[:, :, :, None] * value_heads[:, :, None, :]
    )
    norm_next = decay_rate[:, :, None] * norm_state + injected[:, :, None] * key_heads
    numerator = jnp.einsum(
        "shd,shde->she", query_heads, memory_next, precision=lax.Precision.HIGHEST
    )
    denominator = jnp.maximum(
        jnp.abs(jnp.sum(query_heads * norm_next, axis=-1)), jnp.exp(-max_next)
    )
    readout = numerator / denominator[:, :, None]
    readout = rms_scale(readout, head_gain.reshape(head_count, head_size))
    gated = readout.reshape(row_count, head_count * head_size) * jax.nn.sigmoid(
        outgate.astype(jnp.float32)
    )
    return (gated.astype(jnp.bfloat16), memory_next, norm_next, max_next)


def shards(
    tokens,
    first_gain,
    query_weight,
    key_weight,
    value_weight,
    outgate_weight,
    igate_weight,
    fgate_weight,
    igate_bias,
    fgate_bias,
    memory_state,
    norm_state,
    max_state,
    head_gain,
    out_weight,
    second_gain,
    expert_ids,
    route_weight,
    expert_gate,
    expert_up,
    expert_down,
    shared_gate,
    shared_up,
    shared_down,
):
    own_rows = tokens.shape[0]
    devices = lax.axis_size(EP)
    top_count = expert_ids.shape[1]
    capacity = max(2, 2 * own_rows * top_count // devices)
    inputs = tokens.astype(jnp.float32)
    normed = rms_scale(inputs, first_gain).astype(jnp.bfloat16)
    block_rows = gather_axes(normed, EP, (0, 1), 0)
    columns = jnp.stack(
        [
            jnp.dot(block_rows, matrix, preferred_element_type=jnp.float32).astype(jnp.bfloat16)
            for matrix in (query_weight, key_weight, value_weight, outgate_weight)
        ]
    )
    projected = lax.all_to_all(columns, EP, split_axis=1, concat_axis=2, tiled=True)
    gated, memory_next, norm_next, max_next = cell_step(
        normed,
        projected[0],
        projected[1],
        projected[2],
        projected[3],
        igate_weight,
        fgate_weight,
        igate_bias,
        fgate_bias,
        memory_state,
        norm_state,
        max_state,
        head_gain,
    )
    picked = gated
    mix_sums = jnp.dot(
        picked,
        lax.all_gather(out_weight, EP, axis=0, tiled=True),
        preferred_element_type=jnp.float32,
    )
    stream = inputs + mix_sums.astype(jnp.bfloat16).astype(jnp.float32)
    normed_two = rms_scale(stream, second_gain).astype(jnp.bfloat16)
    block_rows = side_by_side((shared_gate, shared_up), EP, 0, 1)
    picked = normed_two
    gate_shared = jnp.dot(picked, block_rows[0], preferred_element_type=jnp.float32)
    up_shared = jnp.dot(picked, block_rows[1], preferred_element_type=jnp.float32)
    hidden_shared = (jax.nn.silu(gate_shared) * up_shared).astype(jnp.bfloat16)
    shared_result = jnp.dot(
        hidden_shared, gather_axes(shared_down, EP, (0, 1), 1), preferred_element_type=jnp.float32
    )
    choose = (expert_ids[:, :, None] == jnp.arange(devices, dtype=jnp.int32)[None, None, :]).astype(
        jnp.int32
    )
    counted = jnp.sum(choose, axis=1)
    ranking = jnp.cumsum(counted, axis=0) - counted
    slot_index = jnp.sum(choose * ranking[:, None, :], axis=2)
    slot_ids = jnp.arange(capacity, dtype=jnp.int32)
    selector = counted.T[:, None, :] * (ranking.T[:, None, :] == slot_ids[None, :, None]).astype(
        jnp.int32
    )
    outgoing = jnp.einsum(
        "ecr,rd->ecd", selector.astype(jnp.bfloat16), normed_two, preferred_element_type=jnp.float32
    ).astype(jnp.bfloat16)
    arrived = lax.all_to_all(outgoing, EP, split_axis=0, concat_axis=0, tiled=True)
    sources, slots, width = arrived.shape
    flat_rows = arrived.reshape(sources * slots, width)
    gate_sums = jnp.dot(flat_rows, expert_gate[0], preferred_element_type=jnp.float32)
    up_sums = jnp.dot(flat_rows, expert_up[0], preferred_element_type=jnp.float32)
    hidden = (jax.nn.silu(gate_sums) * up_sums).astype(jnp.bfloat16)
    result = jnp.dot(hidden, expert_down[0], preferred_element_type=jnp.float32).astype(
        jnp.bfloat16
    )
    results = lax.all_to_all(
        result.reshape(sources, slots, width), EP, split_axis=0, concat_axis=0, tiled=True
    )
    flat_results = results.reshape(devices * capacity, results.shape[2])
    picked_results = flat_results[expert_ids * capacity + slot_index]
    routed = jnp.sum(route_weight[:, :, None] * picked_results.astype(jnp.float32), axis=1)
    mixed_out = (stream + routed + shared_result).astype(jnp.bfloat16)
    return (mixed_out, memory_next, norm_next, max_next)


def solution(mesh):
    torus = Mesh(mesh.devices.reshape(mesh.shape["grp"], 32, 2), ("grp", "ep_0", "ep_1"))
    placed = (
        P(GRP_EP, None),
        P(),
        P(None, EP),
        P(None, EP),
        P(None, EP),
        P(None, EP),
        P(),
        P(),
        P(),
        P(),
        P(GRP_EP, None, None, None),
        P(GRP_EP, None, None),
        P(GRP_EP, None),
        P(),
        P(EP, None),
        P(),
        P(GRP_EP, None),
        P(GRP_EP, None),
        P(EP, None, None),
        P(EP, None, None),
        P(EP, None, None),
        P(EP, None),
        P(EP, None),
        P(None, EP),
    )
    return jax.shard_map(
        shards,
        mesh=torus,
        in_specs=placed,
        out_specs=(
            P(GRP_EP, None),
            P(GRP_EP, None, None, None),
            P(GRP_EP, None, None),
            P(GRP_EP, None),
        ),
        check_vma=False,
    )
```

profile of v0, /device:TPU:102, one launch (start us, length us, event | category | flops | bytes accessed | tf_op | source)
XLA Modules:
  0.0 611.0 jit_solution(12208696198347227627)
XLA Ops:
  8.0 0.9 fusion.24
  8.9 1.5 fusion.26
  10.5 142.0 %all-gather.16.cloned.1.call-done = bf16[256,2048]{1,0:T(8,128)(2,1)} async-done(((bf16[8,2048]{1,0:T(8,128)(2,1)}), bf16[256,2048]{1,0:T(8,128)(2,1)}) %all-gather.16.cloned.1.call-update) | async-done | bytes 1048592 | tf_op jit(solution)/shard_map/all_gather | solution.py:23
  154.2 0.9 convolution_add_fusion.1
  155.1 19.5 %all-gather.8.cloned.1.call-done = bf16[64,8,2048]{2,1,0:T(8,128)(2,1)} async-done(((bf16[32,8,2048]{2,1,0:T(8,128)(2,1)}), bf16[64,8,2048]{2,1,0:T(8,128)(2,1)}) %all-gather.8.cloned.1.call-update) | async-done | bytes 2097168 | tf_op jit(solution)/shard_map/all_gather | solution.py:23
  174.6 1.8 copy.81
  179.6 1.1 reshape.149
  180.7 23.5 %all-to-all-start = ((bf16[64,2,256]{2,1,0:T(2,128)(2,1)}), bf16[64,2,256]{2,1,0:T(2,128)(2,1)S(1)}, u32[]{:S(2)}, u32[]{:S(2)}) async-start(bf16[64,2,256]{2,1,0:T(2,128)(2,1)} %reshape.149), calls=%async_computation | async-start | bytes 131072 | tf_op jit(solution)/shard_map/all_to_all | solution.py:137
  204.5 25.3 %all-to-all-done = bf16[64,2,256]{2,1,0:T(2,128)(2,1)S(1)} async-done(((bf16[64,2,256]{2,1,0:T(2,128)(2,1)}), bf16[64,2,256]{2,1,0:T(2,128)(2,1)S(1)}, u32[]{:S(2)}, u32[]{:S(2)}) %all-to-all-start) | async-done | bytes 65568 | tf_op jit(solution)/shard_map/all_to_all | solution.py:137
  232.9 3.7 multiply_add_fusion
  236.6 2.0 fusion.47
  238.8 74.3 %all-gather.10.cloned.1.call-done = bf16[1024,2048]{1,0:T(8,128)(2,1)} async-done(((bf16[16,2048]{1,0:T(8,128)(2,1)}), bf16[1024,2048]{1,0:T(8,128)(2,1)}) %all-gather.10.cloned.1.call-update) | async-done | bytes 4194320 | tf_op jit(solution)/shard_map/all_gather | solution.py:156
  313.1 3.0 multiply_reduce_fusion.1
  316.5 1.3 copy.91
  317.8 15.5 %all-to-all-start.1 = ((bf16[64,2,2048]{2,1,0:T(2,128)(2,1)}), bf16[64,2,2048]{2,1,0:T(2,128)(2,1)S(1)}, u32[]{:S(2)}, u32[]{:S(2)}) async-start(bf16[64,2,2048]{2,1,0:T(2,128)(2,1)} %copy.91), calls=%async_computation.1 | async-start | bytes 1048576 | tf_op jit(solution)/shard_map/all_to_all | solution.py:182
  333.4 97.8 %all-gather.1 = bf16[8192,32]{0,1:T(8,128)(2,1)S(1)} all-gather(bf16[256,32]{0,1:T(8,128)(2,1)S(1)} %copy-done.12), channel_id=3, replica_groups=mesh['grp'=4,'ep_0'=32,'ep_1'=2] {'ep_0'}, dimensions={0}, use_global_device_ids=true | all-gather | bytes 540672 | tf_op jit(solution)/shard_map/all_gather | solution.py:23
  431.3 0.9 copy.101
  433.2 1.5 fusion.17
  435.6 1.1 reshape.121
  436.7 22.5 %all-to-all-start.2 = ((bf16[64,2,2048]{2,1,0:T(2,128)(2,1)}), bf16[64,2,2048]{2,1,0:T(2,128)(2,1)S(1)}, u32[]{:S(2)}, u32[]{:S(2)}) async-start(bf16[64,2,2048]{2,1,0:T(2,128)(2,1)} %reshape.121), calls=%async_computation.2 | async-start | bytes 1048576 | tf_op jit(solution)/shard_map/all_to_all | solution.py:191
  459.7 1.8 copy.95
  461.5 137.5 %all-gather.12.cloned.1.call-done = bf16[2048,512]{1,0:T(8,128)(2,1)} async-done(((bf16[32,512]{1,0:T(8,128)(2,1)}), bf16[2048,512]{1,0:T(8,128)(2,1)}) %all-gather.12.cloned.1.call-update) | async-done | bytes 2097168 | tf_op jit(solution)/shard_map/all_gather | solution.py:36
  599.0 1.5 fusion.12
  601.8 2.7 fusion
  (102 shorter events, 13.0 us)
Async XLA Ops:
  7.2 427.6 %copy-start = (bf16[1,256,2048]{2,1,0:T(8,128)(2,1)S(1)}, bf16[1,256,2048]{2,1,0:T(8,128)(2,1)}, u32[]{:S(2)}) copy-start(bf16[1,256,2048]{2,1,0:T(8,128)(2,1)} %param.44) | copy-start | bytes 3145732
  7.2 145.3 %all-gather.16.cloned.1.call-start = ((), (), s32[]{:S(2)}) async-start(), calls=%async_computation.7 | async-start | bytes 1081344 | tf_op jit(solution)/shard_map/all_gather | solution.py:23
  10.4 164.2 %all-gather.8.cloned.1.call-start = ((), (), s32[]{:S(2)}) async-start(), calls=%async_computation.3 | async-start | bytes 3145728 | tf_op jit(solution)/shard_map/all_gather | solution.py:23
  152.5 160.6 %all-gather.10.cloned.1.call-start = ((), (), s32[]{:S(2)}) async-start(), calls=%async_computation.4 | async-start | bytes 4259840 | tf_op jit(solution)/shard_map/all_gather | solution.py:156
  174.6 1.8 copy-start.5
  178.6 25.7 %copy-start.18 = (bf16[1024]{0:T(1024)(128)(2,1)S(1)}, bf16[1024]{0:T(1024)(128)(2,1)}, u32[]{:S(2)}) copy-start(bf16[1024]{0:T(1024)(128)(2,1)} %param.37) | copy-start | bytes 6148
  178.6 25.7 %copy-start.16 = (bf16[2048]{0:T(1024)(128)(2,1)S(1)}, bf16[2048]{0:T(1024)(128)(2,1)}, u32[]{:S(2)}) copy-start(bf16[2048]{0:T(1024)(128)(2,1)} %param.39) | copy-start | bytes 12292
  178.6 25.7 %copy-start.3 = (bf16[8,2048]{1,0:T(8,128)(2,1)S(1)}, bf16[8,2048]{1,0:T(8,128)(2,1)}, u32[]{:S(2)}) copy-start(bf16[8,2048]{1,0:T(8,128)(2,1)} %fusion.26) | copy-start | bytes 98308
  178.6 25.7 %copy-start.11 = (bf16[2048,8]{0,1:T(8,128)(2,1)S(1)}, bf16[2048,8]{0,1:T(8,128)(2,1)}, u32[]{:S(2)}) copy-start(bf16[2048,8]{0,1:T(8,128)(2,1)} %param.31) | copy-start | bytes 98308
  178.6 25.7 %copy-start.17 = (f32[8,8]{1,0:T(8,128)S(1)}, f32[8,8]{1,0:T(8,128)}, u32[]{:S(2)}) copy-start(f32[8,8]{1,0:T(8,128)} %param.36) | copy-start | bytes 772
  178.6 25.7 %copy-start.19 = (f32[8]{0:T(128)S(1)}, f32[8]{0:T(128)}, u32[]{:S(2)}) copy-start(f32[8]{0:T(128)} %param.33) | copy-start | bytes 100
  179.6 52.1 %copy-start.10 = (f32[8,8,128]{2,1,0:T(8,128)S(1)}, f32[8,8,128]{2,1,0:T(8,128)}, u32[]{:S(2)}) copy-start(f32[8,8,128]{2,1,0:T(8,128)} %param.35) | copy-start | bytes 98308
  180.7 49.1 %all-to-all-start = ((bf16[64,2,256]{2,1,0:T(2,128)(2,1)}), bf16[64,2,256]{2,1,0:T(2,128)(2,1)S(1)}, u32[]{:S(2)}, u32[]{:S(2)}) async-start(bf16[64,2,256]{2,1,0:T(2,128)(2,1)} %reshape.149), calls=%async_computation | async-start | bytes 131072 | tf_op jit(solution)/shard_map/all_to_all | solution.py:137
  204.5 32.1 %copy-start.9 = (f32[8,8]{1,0:T(8,128)}, f32[8,8]{1,0:T(8,128)S(1)}, u32[]{:S(2)}) copy-start(f32[8,8]{1,0:T(8,128)S(1)} %get-tuple-element.7) | copy-start | bytes 772
  236.6 2.0 copy-start.1
  236.6 76.5 %copy-start.4 = (bf16[8,2048]{1,0:T(8,128)(2,1)S(1)}, bf16[8,2048]{1,0:T(8,128)(2,1)}, u32[]{:S(2)}) copy-start(bf16[8,2048]{1,0:T(8,128)(2,1)} %param.24) | copy-start | bytes 98308
  316.1 17.3 %copy-start.12 = (bf16[256,32]{0,1:T(8,128)(2,1)S(1)}, bf16[256,32]{0,1:T(8,128)(2,1)}, u32[]{:S(2)}) copy-start(bf16[256,32]{0,1:T(8,128)(2,1)} %param.47) | copy-start | bytes 49156
  316.5 115.8 %copy-start.13 = (bf16[32,256]{1,0:T(8,128)(2,1)S(1)}, bf16[32,256]{1,0:T(8,128)(2,1)}, u32[]{:S(2)}) copy-start(bf16[32,256]{1,0:T(8,128)(2,1)} %param.46) | copy-start | bytes 49156
  316.5 115.8 %copy-start.14 = (bf16[32,256]{1,0:T(8,128)(2,1)S(1)}, bf16[32,256]{1,0:T(8,128)(2,1)}, u32[]{:S(2)}) copy-start(bf16[32,256]{1,0:T(8,128)(2,1)} %param.45) | copy-start | bytes 49156
  317.8 115.2 %all-to-all-start.1 = ((bf16[64,2,2048]{2,1,0:T(2,128)(2,1)}), bf16[64,2,2048]{2,1,0:T(2,128)(2,1)S(1)}, u32[]{:S(2)}, u32[]{:S(2)}) async-start(bf16[64,2,2048]{2,1,0:T(2,128)(2,1)} %copy.91), calls=%async_computation.1 | async-start | bytes 1048576 | tf_op jit(solution)/shard_map/all_to_all | solution.py:182
  333.4 126.3 %all-gather.14.cloned.1.call-start = ((), (), s32[]{:S(2)}) async-start(), calls=%async_computation.6 | async-start | bytes 1572864 | tf_op jit(solution)/shard_map/all_gather | solution.py:23
  431.3 3.5 copy-start.2
  432.2 166.8 %all-gather.12.cloned.1.call-start = ((), (), s32[]{:S(2)}) async-start(), calls=%async_computation.5 | async-start | bytes 2129920 | tf_op jit(solution)/shard_map/all_gather | solution.py:36
  436.7 163.8 %all-to-all-start.2 = ((bf16[64,2,2048]{2,1,0:T(2,128)(2,1)}), bf16[64,2,2048]{2,1,0:T(2,128)(2,1)S(1)}, u32[]{:S(2)}, u32[]{:S(2)}) async-start(bf16[64,2,2048]{2,1,0:T(2,128)(2,1)} %reshape.121), calls=%async_computation.2 | async-start | bytes 1048576 | tf_op jit(solution)/shard_map/all_to_all | solution.py:191
  (4 other events, 4.6 us)
Sparse Core Ops, SparseCore 0:
  10.6 141.8 all-gather.15
  154.3 20.3 all-gather.7
  176.5 136.5 all-gather.9
  432.4 26.4 all-gather.13
  461.1 137.9 all-gather.11
where the time goes:
time: 615 us; the launch traced here: 611 us
  waiting for transfers between devices  400 us (65%)
  blocking collectives  97.8 us (16%)
  starting transfers between devices  61.8 us (10%)
  matrix products  15.5 us (3%)
  between operations  14.3 us (2%)
  local copies, waits for them, and re-layouts  12.9 us (2%)
  other arithmetic  9.01 us (1%)
    all_gather x3, waiting for transfers between devices, stacked_from(): parts = lax.all_gather(parts, axes[k], axis=0, tiled=True)  162 us
    all_gather x1, waiting for transfers between devices, side_by_side(): whole, at, outs = (lax.all_gather(both, axis, axis=dim, tiled=True), 0, [])  138 us
    all_gather x1, blocking collectives, stacked_from(): parts = lax.all_gather(parts, axes[k], axis=0, tiled=True)  97.8 us
    all_gather x1, waiting for transfers between devices, shards(): lax.all_gather(out_weight, EP, axis=0, tiled=True)  74.3 us
    all_to_all x1, waiting for transfers between devices, shards(): lax.all_to_all(columns, EP, split_axis=1, concat_axis=2, tiled=True)  25.3 us
    all_to_all x1, starting transfers between devices, shards(): lax.all_to_all(columns, EP, split_axis=1, concat_axis=2, tiled=True)  23.5 us
    all_to_all x1, starting transfers between devices, shards(): lax.all_to_all(result.reshape(sources, slots, width), EP, split_axis=0, c...  22.5 us
    all_to_all x1, starting transfers between devices, shards(): lax.all_to_all(outgoing, EP, split_axis=0, concat_axis=0, tiled=True)  15.5 us
  transfers between devices with their start and end apart: 8, of which 5 were waited for; matrix products, arithmetic and copies ran while one was open for 4% of the time, Pallas kernels for 0%

commit v1 on v0

v1 whole, which is shorter than its diff:
```python
import jax
import jax.numpy as jnp
from jax import lax
from jax.sharding import Mesh
from jax.sharding import PartitionSpec as P

FAR = "za"
NEAR = ("zb", "core")
RING = ("za", "zb")
EP = ("za", "zb", "core")
GRP_EP = ("grp", "za", "zb", "core")

epsilon = 1e-06


def rms_scale(values, gain):
    return (
        values
        * lax.rsqrt(jnp.mean(values * values, axis=-1, keepdims=True) + epsilon)
        * gain.astype(jnp.float32)
    )


def cell_step(
    normed,
    query,
    key_proj,
    value_proj,
    outgate,
    igate_weight,
    fgate_weight,
    igate_bias,
    fgate_bias,
    memory_state,
    norm_state,
    max_state,
    head_gain,
):
    row_count, head_count = max_state.shape
    head_size = memory_state.shape[-1]
    input_gate = jnp.dot(normed, igate_weight, preferred_element_type=jnp.float32) + igate_bias
    forget_log = jax.nn.log_sigmoid(
        jnp.dot(normed, fgate_weight, preferred_element_type=jnp.float32) + fgate_bias
    )
    query_heads = query.astype(jnp.float32).reshape(row_count, head_count, head_size)
    key_heads = key_proj.astype(jnp.float32).reshape(
        row_count, head_count, head_size
    ) * head_size ** (-0.5)
    value_heads = value_proj.astype(jnp.float32).reshape(row_count, head_count, head_size)
    max_next = jnp.maximum(forget_log + max_state, input_gate)
    decay_rate = jnp.exp(forget_log + max_state - max_next)
    injected = jnp.exp(input_gate - max_next)
    memory_next = decay_rate[:, :, None, None] * memory_state + injected[:, :, None, None] * (
        key_heads[:, :, :, None] * value_heads[:, :, None, :]
    )
    norm_next = decay_rate[:, :, None] * norm_state + injected[:, :, None] * key_heads
    numerator = jnp.einsum(
        "shd,shde->she", query_heads, memory_next, precision=lax.Precision.HIGHEST
    )
    denominator = jnp.maximum(
        jnp.abs(jnp.sum(query_heads * norm_next, axis=-1)), jnp.exp(-max_next)
    )
    readout = numerator / denominator[:, :, None]
    readout = rms_scale(readout, head_gain.reshape(head_count, head_size))
    gated = readout.reshape(row_count, head_count * head_size) * jax.nn.sigmoid(
        outgate.astype(jnp.float32)
    )
    return (gated.astype(jnp.bfloat16), memory_next, norm_next, max_next)


def rounded(values, kind):
    info = jnp.finfo(kind)
    return lax.reduce_precision(values, info.nexp, info.nmant)


def earlier_count(named, axis):
    count = named.shape[axis]
    before = jnp.arange(count)[:, None] < jnp.arange(count)[None, :]
    moved = jnp.moveaxis(named, axis, -1)
    counts = jnp.sum(jnp.where(before, moved[..., :, None], 0.0), axis=-2)
    return jnp.moveaxis(counts, -1, axis)


def split_two(values, kind):
    high = rounded(values, kind)
    return high.astype(kind), (values - high).astype(kind)


def shards(
    tokens,
    first_gain,
    query_weight,
    key_weight,
    value_weight,
    outgate_weight,
    igate_weight,
    fgate_weight,
    igate_bias,
    fgate_bias,
    memory_state,
    norm_state,
    max_state,
    head_gain,
    out_weight,
    second_gain,
    expert_ids,
    route_weight,
    expert_gate,
    expert_up,
    expert_down,
    shared_gate,
    shared_up,
    shared_down,
):
    f32, bf16, f16 = jnp.float32, jnp.bfloat16, jnp.float16
    rows, width = tokens.shape
    top = expert_ids.shape[1]
    far = lax.axis_size(FAR)
    near_z = lax.axis_size("zb")
    cores = lax.axis_size("core")
    near = near_z * cores
    ring = far * near_z
    devices = ring * cores
    slots = max(2, 2 * rows * top // devices)
    my_far = lax.axis_index(FAR)
    my_zb = lax.axis_index("zb")
    my_core = lax.axis_index("core")
    swap = [(i, (i + 1) % cores) for i in range(cores)]

    half = width // 2
    hidden = shared_gate.shape[1]
    packed = jnp.concatenate(
        [
            jnp.concatenate([out_weight[:, :half], out_weight[:, half:]], axis=0),
            shared_gate,
            shared_up,
            shared_down.T,
        ],
        axis=1,
    )
    whole = lax.all_gather(packed, EP, axis=0, tiled=True)

    own = jnp.concatenate([query_weight.T, key_weight.T, value_weight.T, outgate_weight.T], axis=0)
    other = lax.ppermute(own, "core", swap)

    inputs = tokens.astype(f32)
    normed_exact = rounded(rms_scale(inputs, first_gain), bf16)
    normed = normed_exact.astype(bf16)
    weight_high, weight_low = split_two(route_weight, f16)
    notes = jnp.concatenate([expert_ids.astype(f16), weight_high, weight_low], axis=1)
    notes = jnp.pad(notes, ((0, 0), (0, 128 - notes.shape[1])))
    gathered = lax.all_gather(
        jnp.concatenate([normed_exact.astype(f16), notes], axis=1), RING, axis=0, tiled=True
    )
    block_rows = gathered[:, :width].astype(bf16)
    my_notes = gathered[:, width:]
    other_notes = lax.ppermute(my_notes, "core", swap)

    pair = jnp.where(my_core == 0, jnp.stack([own, other]), jnp.stack([other, own]))
    columns = lax.dot_general(
        block_rows, pair.reshape(-1, width), (((1,), (1,)), ((), ())), preferred_element_type=f32
    ).astype(bf16)
    projected = lax.all_to_all(
        columns.reshape(ring, rows, columns.shape[1]), RING, split_axis=0, concat_axis=0, tiled=True
    )
    share = query_weight.shape[1]
    projected = projected.reshape(ring, rows, cores, 4, share).transpose(3, 1, 0, 2, 4)
    projected = projected.reshape(4, rows, devices * share)

    mine = my_notes.reshape(far, near_z, rows, 128)
    theirs = other_notes.reshape(far, near_z, rows, 128)
    both = jnp.where(my_core == 0, jnp.stack([mine, theirs], 2), jnp.stack([theirs, mine], 2))
    me = (my_far * near + my_zb * cores + my_core).astype(f32)
    named = jnp.any(both[..., :top].astype(f32) == me, axis=-1).astype(f32)
    place = earlier_count(named, 3)
    slot_ids = jnp.arange(slots, dtype=f32)
    picks = named[..., None] * (place[..., None] == slot_ids)
    picks = picks.transpose(1, 2, 0, 4, 3).reshape(near, far, slots, rows)
    source = jnp.arange(far)[None, :, None, None] * near + jnp.arange(near)[:, None, None, None]
    selector = jnp.where(
        source[..., None] == jnp.arange(devices)[:, None], picks[:, :, :, None, :], 0.0
    )
    selector = selector.reshape(near * far * slots, devices * rows).astype(bf16)
    at_mine = lax.dynamic_index_in_dim(mine, my_zb, axis=1, keepdims=False).astype(f32)
    block_experts = (my_far * near).astype(f32) + jnp.arange(near, dtype=f32)
    hits = (at_mine[:, :, :top, None] == block_experts).astype(f32)
    weights = at_mine[:, :, top : 2 * top] + at_mine[:, :, 2 * top : 3 * top]
    hit = jnp.sum(hits, axis=2)
    hit_weight = jnp.sum(hits * weights[..., None], axis=2)
    hit_place = earlier_count(hit, 1)
    mixer = hit_weight[..., None] * (hit_place[..., None] == slot_ids) * hit[..., None]
    mixer = jnp.where(
        (jnp.arange(far)[:, None] == jnp.arange(far))[:, None, None, :, None],
        mixer[:, :, :, None, :],
        0.0,
    )
    mixer = mixer.reshape(far * rows, near * far * slots)
    mixer_high, mixer_low = split_two(mixer, bf16)

    gated, memory_next, norm_next, max_next = cell_step(
        normed,
        projected[0],
        projected[1],
        projected[2],
        projected[3],
        igate_weight,
        fgate_weight,
        igate_bias,
        fgate_bias,
        memory_state,
        norm_state,
        max_state,
        head_gain,
    )
    spread = gated.reshape(1, rows, devices, 1, -1) * jnp.eye(2, dtype=bf16).reshape(2, 1, 1, 2, 1)
    mix_sums = jnp.dot(
        spread.reshape(2 * rows, -1), whole[:, :half], preferred_element_type=f32
    )
    mix_sums = jnp.concatenate([mix_sums[:rows], mix_sums[rows:]], axis=1)
    stream = inputs + mix_sums.astype(bf16).astype(f32)
    normed_exact = rounded(rms_scale(stream, second_gain), bf16)
    normed_two = normed_exact.astype(bf16)

    all_rows = lax.all_gather(normed_exact.astype(f16), EP, axis=0, tiled=True).astype(bf16)
    flat_rows = jnp.dot(selector, all_rows, preferred_element_type=f32).astype(bf16)
    gate_sums = jnp.dot(flat_rows, expert_gate[0], preferred_element_type=f32)
    up_sums = jnp.dot(flat_rows, expert_up[0], preferred_element_type=f32)
    hidden_rows = (jax.nn.silu(gate_sums) * up_sums).astype(bf16)
    result = jnp.dot(hidden_rows, expert_down[0], preferred_element_type=f32).astype(bf16)
    near_results = lax.all_to_all(
        result.reshape(near, far * slots, width), NEAR, split_axis=0, concat_axis=0, tiled=True
    ).reshape(near * far * slots, width)
    partial = jnp.dot(mixer_high, near_results, preferred_element_type=f32) + jnp.dot(
        mixer_low, near_results, preferred_element_type=f32
    )
    far_sums = lax.all_to_all(
        partial.astype(bf16).reshape(far, rows, width), FAR, split_axis=0, concat_axis=0, tiled=True
    )
    routed = jnp.sum(far_sums.astype(f32), axis=0)

    gate_up = jnp.dot(normed_two, whole[:, half : half + 2 * hidden], preferred_element_type=f32)
    hidden_shared = (jax.nn.silu(gate_up[:, :hidden]) * gate_up[:, hidden:]).astype(bf16)
    shared_result = lax.dot_general(
        hidden_shared,
        whole[:, half + 2 * hidden :],
        (((1,), (1,)), ((), ())),
        preferred_element_type=f32,
    )
    mixed_out = (stream + routed + shared_result).astype(bf16)
    return (mixed_out, memory_next, norm_next, max_next)


def solution(mesh):
    torus = Mesh(
        mesh.devices.reshape(mesh.shape["grp"], 8, 4, 2), ("grp", "za", "zb", "core")
    )
    placed = (
        P(GRP_EP, None),
        P(),
        P(None, EP),
        P(None, EP),
        P(None, EP),
        P(None, EP),
        P(),
        P(),
        P(),
        P(),
        P(GRP_EP, None, None, None),
        P(GRP_EP, None, None),
        P(GRP_EP, None),
        P(),
        P(EP, None),
        P(),
        P(GRP_EP, None),
        P(GRP_EP, None),
        P(EP, None, None),
        P(EP, None, None),
        P(EP, None, None),
        P(EP, None),
        P(EP, None),
        P(None, EP),
    )
    return jax.shard_map(
        shards,
        mesh=torus,
        in_specs=placed,
        out_specs=(
            P(GRP_EP, None),
            P(GRP_EP, None, None, None),
            P(GRP_EP, None, None),
            P(GRP_EP, None),
        ),
        check_vma=False,
    )
```

time: 615 us -> 309 us (0.50)
  waiting for transfers between devices: 400 us -> 77.7 us
  blocking collectives: 97.8 us -> 139 us
  starting transfers between devices: 61.8 us -> 34.8 us
  other arithmetic: 9.01 us -> 16.4 us
    all_gather x5 -> x1, waiting for transfers between devices: 373 us -> 7.31 us  [shards(): whole = lax.all_gather(packed, EP, axis=0, tiled=True)]
    all_to_all x3, waiting for transfers between devices: 25.3 us -> 70.3 us  [the longest x1 38.1 us: shards(): lax.all_to_all(partial.astype(bf16).reshape(far, rows, width), FAR, split...]
    all_gather x1 -> x2, blocking collectives: 97.8 us -> 139 us  [the longest x1 80.7 us: shards(): lax.all_gather(jnp.concatenate([normed_exact.astype(f16), notes], axis=1)...]
    all_to_all x3, starting transfers between devices: 61.5 us -> 34.4 us  [the longest x1 15.6 us: shards(): lax.all_to_all(columns.reshape(ring, rows, columns.shape[1]), RING, split...]
    dot_general x10 -> x9, matrix products: 12.5 us -> 11.8 us  [the longest x1 2.93 us: shards(): jnp.dot(spread.reshape(2 * rows, -1), whole[:, :half], preferred_element_...]
  transfers between devices with their start and end apart: 8 -> 6, of which waited for: 5 -> 4; matrix products, arithmetic and copies ran while one was open for 4% -> 9% of each run, Pallas kernels for 0% -> 0%
where the time goes in v1:
time: 309 us; the launch traced here: 308 us
  blocking collectives  139 us (45%)
  waiting for transfers between devices  77.7 us (25%)
  starting transfers between devices  34.8 us (11%)
  other arithmetic  16.4 us (5%)
  matrix products  15.7 us (5%)
  between operations  14.5 us (5%)
  local copies, waits for them, and re-layouts  9.3 us (3%)
    all_gather x1, blocking collectives, shards(): lax.all_gather(jnp.concatenate([normed_exact.astype(f16), notes], axis=1)...  80.7 us
    all_gather x1, blocking collectives, shards(): lax.all_gather(normed_exact.astype(f16), EP, axis=0, tiled=True)  58.6 us
    all_to_all x1, waiting for transfers between devices, shards(): lax.all_to_all(partial.astype(bf16).reshape(far, rows, width), FAR, split...  38.1 us
    all_to_all x1, waiting for transfers between devices, shards(): lax.all_to_all(columns.reshape(ring, rows, columns.shape[1]), RING, split...  21.5 us
    all_to_all x1, starting transfers between devices, shards(): lax.all_to_all(columns.reshape(ring, rows, columns.shape[1]), RING, split...  15.6 us
    all_to_all x1, starting transfers between devices, shards(): lax.all_to_all(partial.astype(bf16).reshape(far, rows, width), FAR, split...  13.1 us
    all_to_all x1, waiting for transfers between devices, shards(): lax.all_to_all(result.reshape(near, far * slots, width), NEAR, split_axis...  10.7 us
    all_gather x1, waiting for transfers between devices, shards(): whole = lax.all_gather(packed, EP, axis=0, tiled=True)  7.31 us
  transfers between devices with their start and end apart: 6, of which 4 were waited for; matrix products, arithmetic and copies ran while one was open for 9% of the time, Pallas kernels for 0%

profile of v1, /device:TPU:102, one launch (start us, length us, event | category | flops | bytes accessed | tf_op | source)
XLA Modules:
  0.0 307.7 jit_solution(18352070372618786392)
XLA Ops:
  8.1 1.4 pad_maximum_fusion.3
  9.6 1.0 fusion.57
  14.7 80.7 %all-gather.5 = f16[256,2176]{1,0:T(8,128)(2,1)S(1)} all-gather(f16[8,2176]{1,0:T(8,128)(2,1)S(1)} %pad_maximum_fusion.4), channel_id=1, replica_groups=mesh['grp'=4,'za'=8,'zb'=4,'core'=2] {'za','zb'}, dimensions={0}, use_global_device_ids=true | all-gather | bytes 1148928 | tf_op jit(solution)/shard_map/all_gather | solution.py:152
  96.3 1.0 fusion.46
  97.3 1.0 broadcast_multiply_fusion.2
  99.0 1.2 fusion.22
  100.4 1.1 fusion.9
  101.5 15.6 %all-to-all-start = ((bf16[32,8,128]{2,1,0:T(8,128)(2,1)}), bf16[32,8,128]{2,1,0:T(8,128)(2,1)S(1)}, u32[]{:S(2)}, u32[]{:S(2)}) async-start(bf16[32,8,128]{2,1,0:T(8,128)(2,1)} %fusion.9), calls=%async_computation | async-start | bytes 131072 | tf_op jit(solution)/shard_map/all_to_all | solution.py:163
  118.1 3.0 convert_element_type.215
  121.1 21.5 %all-to-all-done = bf16[32,8,128]{2,1,0:T(8,128)(2,1)S(1)} async-done(((bf16[32,8,128]{2,1,0:T(8,128)(2,1)}), bf16[32,8,128]{2,1,0:T(8,128)(2,1)S(1)}, u32[]{:S(2)}, u32[]{:S(2)}) %all-to-all-start) | async-done | bytes 65568 | tf_op jit(solution)/shard_map/all_to_all | solution.py:163
  145.1 3.7 %multiply_add_fusion = f32[8,8,128,128]{3,2,1,0:T(8,128)S(1)} fusion(f32[8,8,128,128]{3,2,1,0:T(8,128)} %param.34, f32[8,8,128]{2,1,0:T(8,128)S(1)} %reshape.258, f32[8,8,128]{2,1,0:T(8,128)S(1)} %get-tuple-element.22, f32[8,8]{1,0:T(8,128)S(1)} %get-tuple-element.9, f32[8,8]{1,0:T(8,128)S(1)} %subtract_exponential_fusion.1), kind=kLoop, calls=%fused_computation.3 | loop fusion | flops 4194304 | bytes 8454656 | tf_op jit(solution)/shard_map/add | solution.py:53
  148.9 2.0 copy-done.1
  150.9 2.0 fusion.62
  154.6 7.3 %all-gather.4.cloned.1.call-done = bf16[2048,1792]{1,0:T(8,128)(2,1)} async-done(((bf16[32,1792]{1,0:T(8,128)(2,1)}), bf16[2048,1792]{1,0:T(8,128)(2,1)}) %all-gather.4.cloned.1.call-update) | async-done | bytes 7340048 | tf_op jit(solution)/shard_map/all_gather | solution.py:141
  161.9 2.9 fusion.10
  165.1 58.6 %all-gather.6 = f16[512,2048]{1,0:T(8,128)(2,1)S(1)} all-gather(f16[8,2048]{1,0:T(8,128)(2,1)S(1)} %fusion.38), channel_id=1, replica_groups=mesh['grp'=4,'za'=8,'zb'=4,'core'=2] {'za','zb','core'}, dimensions={0}, use_global_device_ids=true | all-gather | bytes 2129920 | tf_op jit(solution)/shard_map/all_gather | solution.py:224
  224.6 1.6 convolution_convert_fusion
  226.1 5.8 %all-to-all-start.1 = ((bf16[8,16,2048]{2,1,0:T(8,128)(2,1)}), bf16[8,16,2048]{2,1,0:T(8,128)(2,1)S(1)}, u32[]{:S(2)}, u32[]{:S(2)}) async-start(bf16[8,16,2048]{2,1,0:T(8,128)(2,1)} %bitcast.30), calls=%async_computation.1 | async-start | bytes 1048576 | tf_op jit(solution)/shard_map/all_to_all | solution.py:230
  233.5 10.7 %all-to-all-done.1 = bf16[8,16,2048]{2,1,0:T(8,128)(2,1)S(1)} async-done(((bf16[8,16,2048]{2,1,0:T(8,128)(2,1)}), bf16[8,16,2048]{2,1,0:T(8,128)(2,1)S(1)}, u32[]{:S(2)}, u32[]{:S(2)}) %all-to-all-start.1) | async-done | bytes 524320 | tf_op jit(solution)/shard_map/all_to_all | solution.py:230
  244.4 1.0 fusion.3
  245.3 13.1 %all-to-all-start.2 = ((bf16[8,8,2048]{2,1,0:T(8,128)(2,1)}), bf16[8,8,2048]{2,1,0:T(8,128)(2,1)S(1)}, u32[]{:S(2)}, u32[]{:S(2)}) async-start(bf16[8,8,2048]{2,1,0:T(8,128)(2,1)} %fusion.3), calls=%async_computation.2 | async-start | bytes 524288 | tf_op jit(solution)/shard_map/all_to_all | solution.py:236
  258.4 2.0 fusion.5
  260.4 38.1 %all-to-all-done.2 = bf16[8,8,2048]{2,1,0:T(8,128)(2,1)S(1)} async-done(((bf16[8,8,2048]{2,1,0:T(8,128)(2,1)}), bf16[8,8,2048]{2,1,0:T(8,128)(2,1)S(1)}, u32[]{:S(2)}, u32[]{:S(2)}) %all-to-all-start.2) | async-done | bytes 262176 | tf_op jit(solution)/shard_map/all_to_all | solution.py:236
  298.6 2.2 fusion.4
  (89 shorter events, 14.8 us)
Async XLA Ops:
  7.2 217.4 %copy-start = (bf16[1,256,2048]{2,1,0:T(8,128)(2,1)S(1)}, bf16[1,256,2048]{2,1,0:T(8,128)(2,1)}, u32[]{:S(2)}) copy-start(bf16[1,256,2048]{2,1,0:T(8,128)(2,1)} %param.44) | copy-start | bytes 3145732
  7.2 154.7 %all-gather.4.cloned.1.call-start = ((), (), s32[]{:S(2)}) async-start(), calls=%async_computation.3 | async-start | bytes 7454720 | tf_op jit(solution)/shard_map/all_gather | solution.py:141
  10.6 89.7 %collective-permute-start = (bf16[64,2048]{1,0:T(8,128)(2,1)S(1)}, bf16[64,2048]{1,0:T(8,128)(2,1)S(1)}, u32[]{:S(2)}, u32[]{:S(2)}) collective-permute-start(bf16[64,2048]{1,0:T(8,128)(2,1)S(1)} %get-tuple-element.15), channel_id=1, source_target_pairs={{0,1},{1,0},{2,3},{3,2},{4,5},{5,4},{6,7},{7,6},{8,9},{9,8},{10,11... | collective-permute-start | bytes 786440 | tf_op jit(solution)/shard_map/ppermute | solution.py:144
  95.4 3.7 %collective-permute-start.1 = (f16[256,128]{1,0:T(8,128)(2,1)S(1)}, f16[256,128]{1,0:T(8,128)(2,1)S(1)}, u32[]{:S(2)}, u32[]{:S(2)}) collective-permute-start(f16[256,128]{1,0:T(8,128)(2,1)S(1)} %slice.90), channel_id=1, source_target_pairs={{0,1},{1,0},{2,3},{3,2},{4,5},{5,4},{6,7},{7,6},{8,9},{9,8},{10,11... | collective-permute-start | bytes 196616 | tf_op jit(solution)/shard_map/ppermute | solution.py:157
  98.3 46.8 %copy-start.6 = (f32[8,8]{1,0:T(8,128)}, f32[8,8]{1,0:T(8,128)S(1)}, u32[]{:S(2)}) copy-start(f32[8,8]{1,0:T(8,128)S(1)} %get-tuple-element.10) | copy-start | bytes 772
  101.5 42.9 %copy-start.5 = (f32[8,8,128]{2,1,0:T(8,128)S(1)}, f32[8,8,128]{2,1,0:T(8,128)}, u32[]{:S(2)}) copy-start(f32[8,8,128]{2,1,0:T(8,128)} %param.35) | copy-start | bytes 98308
  101.5 41.2 %all-to-all-start = ((bf16[32,8,128]{2,1,0:T(8,128)(2,1)}), bf16[32,8,128]{2,1,0:T(8,128)(2,1)S(1)}, u32[]{:S(2)}, u32[]{:S(2)}) async-start(bf16[32,8,128]{2,1,0:T(8,128)(2,1)} %fusion.9), calls=%async_computation | async-start | bytes 131072 | tf_op jit(solution)/shard_map/all_to_all | solution.py:163
  148.9 2.0 copy-start.1
  152.9 12.0 %copy-start.2 = (bf16[8,2048]{1,0:T(8,128)(2,1)S(1)}, bf16[8,2048]{1,0:T(8,128)(2,1)}, u32[]{:S(2)}) copy-start(bf16[8,2048]{1,0:T(8,128)(2,1)} %param.24) | copy-start | bytes 98308
  161.9 62.3 %copy-start.4 = (bf16[1,2048,256]{2,1,0:T(8,128)(2,1)S(1)}, bf16[1,2048,256]{2,1,0:T(8,128)(2,1)}, u32[]{:S(2)}) copy-start(bf16[1,2048,256]{2,1,0:T(8,128)(2,1)} %param.42) | copy-start | bytes 3145732
  164.9 59.7 %copy-start.3 = (bf16[1,2048,256]{2,1,0:T(8,128)(2,1)S(1)}, bf16[1,2048,256]{2,1,0:T(8,128)(2,1)}, u32[]{:S(2)}) copy-start(bf16[1,2048,256]{2,1,0:T(8,128)(2,1)} %param.43) | copy-start | bytes 3145732
  226.1 18.0 %all-to-all-start.1 = ((bf16[8,16,2048]{2,1,0:T(8,128)(2,1)}), bf16[8,16,2048]{2,1,0:T(8,128)(2,1)S(1)}, u32[]{:S(2)}, u32[]{:S(2)}) async-start(bf16[8,16,2048]{2,1,0:T(8,128)(2,1)} %bitcast.30), calls=%async_computation.1 | async-start | bytes 1048576 | tf_op jit(solution)/shard_map/all_to_all | solution.py:230
  245.3 53.2 %all-to-all-start.2 = ((bf16[8,8,2048]{2,1,0:T(8,128)(2,1)}), bf16[8,8,2048]{2,1,0:T(8,128)(2,1)S(1)}, u32[]{:S(2)}, u32[]{:S(2)}) async-start(bf16[8,8,2048]{2,1,0:T(8,128)(2,1)} %fusion.3), calls=%async_computation.2 | async-start | bytes 524288 | tf_op jit(solution)/shard_map/all_to_all | solution.py:236
Sparse Core Ops, SparseCore 0:
  9.9 152.0 all-gather.3

commit v2 on v1

--- a/solution.py
+++ b/solution.py
@@ -127,19 +127,6 @@
     my_core = lax.axis_index("core")
     swap = [(i, (i + 1) % cores) for i in range(cores)]
 
-    half = width // 2
-    hidden = shared_gate.shape[1]
-    packed = jnp.concatenate(
-        [
-            jnp.concatenate([out_weight[:, :half], out_weight[:, half:]], axis=0),
-            shared_gate,
-            shared_up,
-            shared_down.T,
-        ],
-        axis=1,
-    )
-    whole = lax.all_gather(packed, EP, axis=0, tiled=True)
-
     own = jnp.concatenate([query_weight.T, key_weight.T, value_weight.T, outgate_weight.T], axis=0)
     other = lax.ppermute(own, "core", swap)
 
@@ -148,13 +135,33 @@
     normed = normed_exact.astype(bf16)
     weight_high, weight_low = split_two(route_weight, f16)
     notes = jnp.concatenate([expert_ids.astype(f16), weight_high, weight_low], axis=1)
-    notes = jnp.pad(notes, ((0, 0), (0, 128 - notes.shape[1])))
-    gathered = lax.all_gather(
-        jnp.concatenate([normed_exact.astype(f16), notes], axis=1), RING, axis=0, tiled=True
-    )
-    block_rows = gathered[:, :width].astype(bf16)
-    my_notes = gathered[:, width:]
-    other_notes = lax.ppermute(my_notes, "core", swap)
+    half = width // 2
+    hidden = shared_gate.shape[1]
+    cut = shared_gate.shape[0] // rows
+    piece = width // cut
+    notes = jnp.pad(notes, ((0, (cut - 1) * rows), (0, 128 - notes.shape[1])))
+    payload = jnp.concatenate(
+        [
+            jnp.concatenate(
+                [normed_exact[:, i * piece : (i + 1) * piece] for i in range(cut)], axis=0
+            ).astype(f16),
+            jnp.concatenate([out_weight[:, :half], out_weight[:, half:]], axis=0).astype(f16),
+            shared_gate.astype(f16),
+            shared_up.astype(f16),
+            shared_down.T.astype(f16),
+            notes,
+        ],
+        axis=1,
+    )
+    gathered = lax.all_gather(payload, EP, axis=0, tiled=True)
+    whole = gathered[:, piece : piece + half + 3 * hidden]
+    chips_rows = gathered[:, :piece].reshape(ring, cores, cut, rows, piece)
+    chips_rows = lax.dynamic_index_in_dim(chips_rows, my_core, axis=1, keepdims=False)
+    block_rows = chips_rows.transpose(0, 2, 1, 3).reshape(ring * rows, width).astype(bf16)
+    my_notes = gathered[:, piece + half + 3 * hidden :].reshape(far, near, cut * rows, 128)
+    my_notes = lax.dynamic_index_in_dim(
+        my_notes[:, :, :rows], my_zb * cores + my_core, axis=1, keepdims=False
+    ).astype(f32)
 
     pair = jnp.where(my_core == 0, jnp.stack([own, other]), jnp.stack([other, own]))
     columns = lax.dot_general(
@@ -167,35 +174,21 @@
     projected = projected.reshape(ring, rows, cores, 4, share).transpose(3, 1, 0, 2, 4)
     projected = projected.reshape(4, rows, devices * share)
 
-    mine = my_notes.reshape(far, near_z, rows, 128)
-    theirs = other_notes.reshape(far, near_z, rows, 128)
-    both = jnp.where(my_core == 0, jnp.stack([mine, theirs], 2), jnp.stack([theirs, mine], 2))
-    me = (my_far * near + my_zb * cores + my_core).astype(f32)
-    named = jnp.any(both[..., :top].astype(f32) == me, axis=-1).astype(f32)
-    place = earlier_count(named, 3)
     slot_ids = jnp.arange(slots, dtype=f32)
-    picks = named[..., None] * (place[..., None] == slot_ids)
-    picks = picks.transpose(1, 2, 0, 4, 3).reshape(near, far, slots, rows)
-    source = jnp.arange(far)[None, :, None, None] * near + jnp.arange(near)[:, None, None, None]
-    selector = jnp.where(
-        source[..., None] == jnp.arange(devices)[:, None], picks[:, :, :, None, :], 0.0
-    )
-    selector = selector.reshape(near * far * slots, devices * rows).astype(bf16)
-    at_mine = lax.dynamic_index_in_dim(mine, my_zb, axis=1, keepdims=False).astype(f32)
+    at_mine = my_notes
     block_experts = (my_far * near).astype(f32) + jnp.arange(near, dtype=f32)
     hits = (at_mine[:, :, :top, None] == block_experts).astype(f32)
     weights = at_mine[:, :, top : 2 * top] + at_mine[:, :, 2 * top : 3 * top]
     hit = jnp.sum(hits, axis=2)
     hit_weight = jnp.sum(hits * weights[..., None], axis=2)
     hit_place = earlier_count(hit, 1)
-    mixer = hit_weight[..., None] * (hit_place[..., None] == slot_ids) * hit[..., None]
-    mixer = jnp.where(
-        (jnp.arange(far)[:, None] == jnp.arange(far))[:, None, None, :, None],
-        mixer[:, :, :, None, :],
-        0.0,
-    )
-    mixer = mixer.reshape(far * rows, near * far * slots)
+    chosen = (hit_place[..., None] == slot_ids) * hit[..., None]
+    same = (jnp.arange(far)[:, None] == jnp.arange(far))[:, None, None, :, None]
+    chosen = jnp.where(same, chosen[:, :, :, None, :], 0.0)
+    chosen = chosen.reshape(far * rows, near, far * slots)
+    mixer = (chosen * hit_weight.reshape(far * rows, near, 1)).reshape(far * rows, -1)
     mixer_high, mixer_low = split_two(mixer, bf16)
+    selector = chosen.reshape(far * rows, -1).astype(bf16)
 
     gated, memory_next, norm_next, max_next = cell_step(
         normed,
@@ -214,15 +207,19 @@
     )
     spread = gated.reshape(1, rows, devices, 1, -1) * jnp.eye(2, dtype=bf16).reshape(2, 1, 1, 2, 1)
     mix_sums = jnp.dot(
-        spread.reshape(2 * rows, -1), whole[:, :half], preferred_element_type=f32
+        spread.reshape(2 * rows, -1), whole[:, :half].astype(bf16), preferred_element_type=f32
     )
     mix_sums = jnp.concatenate([mix_sums[:rows], mix_sums[rows:]], axis=1)
     stream = inputs + mix_sums.astype(bf16).astype(f32)
-    normed_exact = rounded(rms_scale(stream, second_gain), bf16)
-    normed_two = normed_exact.astype(bf16)
-
-    all_rows = lax.all_gather(normed_exact.astype(f16), EP, axis=0, tiled=True).astype(bf16)
-    flat_rows = jnp.dot(selector, all_rows, preferred_element_type=f32).astype(bf16)
+    normed_two = rounded(rms_scale(stream, second_gain), bf16).astype(bf16)
+
+    far_rows = lax.all_gather(normed_two, FAR, axis=0, tiled=True)
+    outgoing = lax.dot_general(
+        selector, far_rows, (((0,), (0,)), ((), ())), preferred_element_type=f32
+    ).astype(bf16)
+    flat_rows = lax.all_to_all(
+        outgoing.reshape(near, far * slots, width), NEAR, split_axis=0, concat_axis=0, tiled=True
+    ).reshape(near * far * slots, width)
     gate_sums = jnp.dot(flat_rows, expert_gate[0], preferred_element_type=f32)
     up_sums = jnp.dot(flat_rows, expert_up[0], preferred_element_type=f32)
     hidden_rows = (jax.nn.silu(gate_sums) * up_sums).astype(bf16)
@@ -238,11 +235,13 @@
     )
     routed = jnp.sum(far_sums.astype(f32), axis=0)
 
-    gate_up = jnp.dot(normed_two, whole[:, half : half + 2 * hidden], preferred_element_type=f32)
+    gate_up = jnp.dot(
+        normed_two, whole[:, half : half + 2 * hidden].astype(bf16), preferred_element_type=f32
+    )
     hidden_shared = (jax.nn.silu(gate_up[:, :hidden]) * gate_up[:, hidden:]).astype(bf16)
     shared_result = lax.dot_general(
         hidden_shared,
-        whole[:, half + 2 * hidden :],
+        whole[:, half + 2 * hidden :].astype(bf16),
         (((1,), (1,)), ((), ())),
         preferred_element_type=f32,
     )

time: 309 us -> 316 us (1.023)
  blocking collectives: 139 us -> 162 us
  between operations: 14.5 us -> 1.02 us
  starting transfers between devices: 34.8 us -> 30.1 us
  waiting for transfers between devices: 77.7 us -> 73.6 us
    all_to_all x0 -> x1, blocking collectives: none -> 16.9 us  [shards(): lax.all_to_all(outgoing.reshape(near, far * slots, width), NEAR, split_ax...]
    all_gather x1 -> x0, waiting for transfers between devices: 7.31 us -> none  [shards(): whole = lax.all_gather(packed, EP, axis=0, tiled=True)]
    all_gather x2, blocking collectives: 139 us -> 145 us  [the longest x1 109 us: shards(): gathered = lax.all_gather(payload, EP, axis=0, tiled=True)]
    convert_element_type x4 -> x1, local copies, waits for them, and re-layouts: 3.35 us -> 0.19 us  [shards(): selector = chosen.reshape(far * rows, -1).astype(bf16)]
  transfers between devices with their start and end apart: 6 -> 4, of which waited for: 4 -> 3; matrix products, arithmetic and copies ran while one was open for 9% -> 5% of each run, Pallas kernels for 0% -> 0%
where the time goes in v2:
time: 316 us; the launch traced here: 315 us
  blocking collectives  162 us (51%)
  waiting for transfers between devices  73.6 us (23%)
  starting transfers between devices  30.1 us (10%)
  other arithmetic  18.1 us (6%)
  matrix products  18 us (6%)
  local copies, waits for them, and re-layouts  11.8 us (4%)
    all_gather x1, blocking collectives, shards(): gathered = lax.all_gather(payload, EP, axis=0, tiled=True)  109 us
    all_to_all x1, waiting for transfers between devices, shards(): lax.all_to_all(partial.astype(bf16).reshape(far, rows, width), FAR, split...  38.2 us
    all_gather x1, blocking collectives, shards(): far_rows = lax.all_gather(normed_two, FAR, axis=0, tiled=True)  36.6 us
    all_to_all x1, waiting for transfers between devices, shards(): lax.all_to_all(columns.reshape(ring, rows, columns.shape[1]), RING, split...  23.7 us
    all_to_all x1, blocking collectives, shards(): lax.all_to_all(outgoing.reshape(near, far * slots, width), NEAR, split_ax...  16.9 us
    all_to_all x1, starting transfers between devices, shards(): lax.all_to_all(columns.reshape(ring, rows, columns.shape[1]), RING, split...  12.9 us
    all_to_all x1, waiting for transfers between devices, shards(): lax.all_to_all(result.reshape(near, far * slots, width), NEAR, split_axis...  11.7 us
    all_to_all x1, starting transfers between devices, shards(): lax.all_to_all(partial.astype(bf16).reshape(far, rows, width), FAR, split...  11.5 us
  transfers between devices with their start and end apart: 4, of which 3 were waited for; matrix products, arithmetic and copies ran while one was open for 5% of the time, Pallas kernels for 0%

profile of v2, /device:TPU:102, one launch (start us, length us, event | category | flops | bytes accessed | tf_op | source)
XLA Modules:
  0.0 315.1 jit_solution(5518528597070664742)
XLA Ops:
  0.6 1.9 fusion.60
  9.5 108.8 %all-gather.1 = f16[2048,2432]{1,0:T(8,128)(2,1)S(1)} all-gather(f16[32,2432]{1,0:T(8,128)(2,1)S(1)} %constant_dynamic-update-slice_fusion), channel_id=1, replica_groups=mesh['grp'=4,'za'=8,'zb'=4,'core'=2] {'za','zb','core'}, dimensions={0}, use_global_device_ids=true | all-gather | bytes 10117120 | tf_op jit(solution)/shard_map/all_gather | solution.py:156
  118.3 1.0 slice.118
  119.3 2.9 copy-done.1
  124.8 1.2 dynamic-slice_convert_fusion
  127.8 1.3 maximum_select_fusion
  129.1 2.3 fusion.7
  131.4 12.9 %all-to-all-start = ((bf16[32,8,128]{2,1,0:T(8,128)(2,1)}), bf16[32,8,128]{2,1,0:T(8,128)(2,1)S(1)}, u32[]{:S(2)}, u32[]{:S(2)}) async-start(bf16[32,8,128]{2,1,0:T(8,128)(2,1)} %fusion.7), calls=%async_computation | async-start | bytes 131072 | tf_op jit(solution)/shard_map/all_to_all | solution.py:170
  145.3 23.7 %all-to-all-done = bf16[32,8,128]{2,1,0:T(8,128)(2,1)S(1)} async-done(((bf16[32,8,128]{2,1,0:T(8,128)(2,1)}), bf16[32,8,128]{2,1,0:T(8,128)(2,1)S(1)}, u32[]{:S(2)}, u32[]{:S(2)}) %all-to-all-start) | async-done | bytes 65568 | tf_op jit(solution)/shard_map/all_to_all | solution.py:170
  170.2 1.5 multiply_reduce_fusion.2
  172.3 3.7 %multiply_add_fusion = f32[8,8,128,128]{3,2,1,0:T(8,128)S(1)} fusion(f32[8,8,128,128]{3,2,1,0:T(8,128)} %param.34, f32[8,8,128]{2,1,0:T(8,128)S(1)} %reshape.215, f32[8,8,128]{2,1,0:T(8,128)S(1)} %get-tuple-element.20, f32[8,8]{1,0:T(8,128)S(1)} %get-tuple-element.9, f32[8,8]{1,0:T(8,128)S(1)} %subtract_exponential_fusion.1), kind=kLoop, calls=%fused_computation.2 | loop fusion | flops 4194304 | bytes 8454656 | tf_op jit(solution)/shard_map/add | solution.py:53
  176.1 2.0 copy-done.2
  178.1 2.0 fusion.65
  181.8 2.9 fusion.8
  185.0 36.6 %all_gather.7 = bf16[64,2048]{1,0:T(8,128)(2,1)S(1)} all-gather(bf16[8,2048]{1,0:T(8,128)(2,1)S(1)} %reduce-precision_convert_fusion.1), channel_id=1, replica_groups=mesh['grp'=4,'za'=8,'zb'=4,'core'=2] {'za'}, dimensions={0}, use_global_device_ids=true | all-gather | bytes 294912 | tf_op jit(solution)/shard_map/all_gather | solution.py:216
  221.9 16.9 %all_to_all.20 = bf16[8,16,2048]{2,1,0:T(8,128)(2,1)S(1)} all-to-all(bf16[8,16,2048]{2,1,0:T(8,128)(2,1)S(1)} %bitcast.90), channel_id=1, replica_groups=mesh['grp'=4,'za'=8,'zb'=4,'core'=2] {'zb','core'}, dimensions={0} | all-to-all | bytes 1048576 | tf_op jit(solution)/shard_map/all_to_all | solution.py:220
  238.8 1.5 fusion.13
  240.4 1.6 convolution_convert_fusion
  241.9 5.7 %all-to-all-start.2 = ((bf16[8,16,2048]{2,1,0:T(8,128)(2,1)}), bf16[8,16,2048]{2,1,0:T(8,128)(2,1)S(1)}, u32[]{:S(2)}, u32[]{:S(2)}) async-start(bf16[8,16,2048]{2,1,0:T(8,128)(2,1)} %bitcast.31), calls=%async_computation.2 | async-start | bytes 1048576 | tf_op jit(solution)/shard_map/all_to_all | solution.py:227
  248.2 11.7 %all-to-all-done.2 = bf16[8,16,2048]{2,1,0:T(8,128)(2,1)S(1)} async-done(((bf16[8,16,2048]{2,1,0:T(8,128)(2,1)}), bf16[8,16,2048]{2,1,0:T(8,128)(2,1)S(1)}, u32[]{:S(2)}, u32[]{:S(2)}) %all-to-all-start.2) | async-done | bytes 524320 | tf_op jit(solution)/shard_map/all_to_all | solution.py:227
  261.1 11.5 %all-to-all-start.3 = ((bf16[8,8,2048]{2,1,0:T(8,128)(2,1)}), bf16[8,8,2048]{2,1,0:T(8,128)(2,1)S(1)}, u32[]{:S(2)}, u32[]{:S(2)}) async-start(bf16[8,8,2048]{2,1,0:T(8,128)(2,1)} %fusion.3), calls=%async_computation.3 | async-start | bytes 524288 | tf_op jit(solution)/shard_map/all_to_all | solution.py:233
  272.6 2.0 fusion.5
  274.6 38.2 %all-to-all-done.3 = bf16[8,8,2048]{2,1,0:T(8,128)(2,1)S(1)} async-done(((bf16[8,8,2048]{2,1,0:T(8,128)(2,1)}), bf16[8,8,2048]{2,1,0:T(8,128)(2,1)S(1)}, u32[]{:S(2)}, u32[]{:S(2)}) %all-to-all-start.3) | async-done | bytes 262176 | tf_op jit(solution)/shard_map/all_to_all | solution.py:233
  312.8 2.3 fusion.4
  (85 shorter events, 17.8 us)
Async XLA Ops:
  0.6 239.7 %copy-start = (bf16[1,256,2048]{2,1,0:T(8,128)(2,1)S(1)}, bf16[1,256,2048]{2,1,0:T(8,128)(2,1)}, u32[]{:S(2)}) copy-start(bf16[1,256,2048]{2,1,0:T(8,128)(2,1)} %param.44) | copy-start | bytes 3145732
  2.5 125.3 %collective-permute-start = (bf16[64,2048]{1,0:T(8,128)(2,1)}, bf16[64,2048]{1,0:T(8,128)(2,1)}, u32[]{:S(2)}, u32[]{:S(2)}) collective-permute-start(bf16[64,2048]{1,0:T(8,128)(2,1)} %get-tuple-element.15), channel_id=1, source_target_pairs={{0,1},{1,0},{2,3},{3,2},{4,5},{5,4},{6,7},{7,6},{8,9},{9,8},{10,11... | collective-permute-start | bytes 786440 | tf_op jit(solution)/shard_map/ppermute | solution.py:131
  3.4 114.9 %copy-start.7 = (f32[8]{0:T(128)}, f32[8]{0:T(128)S(1)}, u32[]{:S(2)}) copy-start(f32[8]{0:T(128)S(1)} %add_rsqrt_fusion.2) | copy-start | bytes 100
  118.3 4.0 %copy-start.1 = (f16[2048,2432]{1,0:T(8,128)(2,1)}, f16[2048,2432]{1,0:T(8,128)(2,1)S(1)}, u32[]{:S(2)}) copy-start(f16[2048,2432]{1,0:T(8,128)(2,1)S(1)} %all-gather.1) | copy-start | bytes 29884420
  118.3 4.5 %copy-start.6 = (bf16[1024]{0:T(1024)(128)(2,1)S(1)}, bf16[1024]{0:T(1024)(128)(2,1)}, u32[]{:S(2)}) copy-start(bf16[1024]{0:T(1024)(128)(2,1)} %param.37) | copy-start | bytes 6148
  122.3 4.5 %copy-start.4 = (bf16[8,2048]{1,0:T(8,128)(2,1)S(1)}, bf16[8,2048]{1,0:T(8,128)(2,1)}, u32[]{:S(2)}) copy-start(bf16[8,2048]{1,0:T(8,128)(2,1)} %param.24) | copy-start | bytes 98308
  131.4 37.7 %all-to-all-start = ((bf16[32,8,128]{2,1,0:T(8,128)(2,1)}), bf16[32,8,128]{2,1,0:T(8,128)(2,1)S(1)}, u32[]{:S(2)}, u32[]{:S(2)}) async-start(bf16[32,8,128]{2,1,0:T(8,128)(2,1)} %fusion.7), calls=%async_computation | async-start | bytes 131072 | tf_op jit(solution)/shard_map/all_to_all | solution.py:170
  145.3 30.7 %copy-start.5 = (f32[8,8]{1,0:T(8,128)}, f32[8,8]{1,0:T(8,128)S(1)}, u32[]{:S(2)}) copy-start(f32[8,8]{1,0:T(8,128)S(1)} %get-tuple-element.10) | copy-start | bytes 772
  176.0 2.0 copy-start.2
  181.8 58.5 %copy-start.3 = (bf16[1,2048,256]{2,1,0:T(8,128)(2,1)S(1)}, bf16[1,2048,256]{2,1,0:T(8,128)(2,1)}, u32[]{:S(2)}) copy-start(bf16[1,2048,256]{2,1,0:T(8,128)(2,1)} %param.43) | copy-start | bytes 3145732
  241.9 17.9 %all-to-all-start.2 = ((bf16[8,16,2048]{2,1,0:T(8,128)(2,1)}), bf16[8,16,2048]{2,1,0:T(8,128)(2,1)S(1)}, u32[]{:S(2)}, u32[]{:S(2)}) async-start(bf16[8,16,2048]{2,1,0:T(8,128)(2,1)} %bitcast.31), calls=%async_computation.2 | async-start | bytes 1048576 | tf_op jit(solution)/shard_map/all_to_all | solution.py:227
  261.1 51.6 %all-to-all-start.3 = ((bf16[8,8,2048]{2,1,0:T(8,128)(2,1)}), bf16[8,8,2048]{2,1,0:T(8,128)(2,1)S(1)}, u32[]{:S(2)}, u32[]{:S(2)}) async-start(bf16[8,8,2048]{2,1,0:T(8,128)(2,1)} %fusion.3), calls=%async_computation.3 | async-start | bytes 524288 | tf_op jit(solution)/shard_map/all_to_all | solution.py:233

commit v3 on v2

--- a/solution.py
+++ b/solution.py
@@ -5,10 +5,10 @@
 from jax.sharding import PartitionSpec as P
 
 FAR = "za"
-NEAR = ("zb", "core")
-RING = ("za", "zb")
-EP = ("za", "zb", "core")
-GRP_EP = ("grp", "za", "zb", "core")
+NEAR = ("zm", "zb", "core")
+ROW = ("za", "zm")
+EP = ("za", "zm", "zb", "core")
+GRP_EP = ("grp", "za", "zm", "zb", "core")
 
 epsilon = 1e-06
 
@@ -71,6 +71,16 @@
 def rounded(values, kind):
     info = jnp.finfo(kind)
     return lax.reduce_precision(values, info.nexp, info.nmant)
+
+
+def from_peer(values, axis):
+    return lax.ppermute(values, axis, [(0, 1), (1, 0)])
+
+
+def in_order(values, axis_names, first):
+    for place, name in enumerate(axis_names, first):
+        values = jnp.where(lax.axis_index(name) == 0, values, jnp.flip(values, place))
+    return values
 
 
 def earlier_count(named, axis):
@@ -116,66 +126,62 @@
     rows, width = tokens.shape
     top = expert_ids.shape[1]
     far = lax.axis_size(FAR)
-    near_z = lax.axis_size("zb")
-    cores = lax.axis_size("core")
-    near = near_z * cores
-    ring = far * near_z
-    devices = ring * cores
+    near = lax.axis_size(NEAR)
+    row = lax.axis_size(ROW)
+    devices = far * near
+    members = devices // row
     slots = max(2, 2 * rows * top // devices)
     my_far = lax.axis_index(FAR)
-    my_zb = lax.axis_index("zb")
-    my_core = lax.axis_index("core")
-    swap = [(i, (i + 1) % cores) for i in range(cores)]
+    share = query_weight.shape[1]
 
     own = jnp.concatenate([query_weight.T, key_weight.T, value_weight.T, outgate_weight.T], axis=0)
-    other = lax.ppermute(own, "core", swap)
+    beside = from_peer(own, "zb")
 
     inputs = tokens.astype(f32)
     normed_exact = rounded(rms_scale(inputs, first_gain), bf16)
     normed = normed_exact.astype(bf16)
     weight_high, weight_low = split_two(route_weight, f16)
     notes = jnp.concatenate([expert_ids.astype(f16), weight_high, weight_low], axis=1)
-    half = width // 2
-    hidden = shared_gate.shape[1]
-    cut = shared_gate.shape[0] // rows
-    piece = width // cut
-    notes = jnp.pad(notes, ((0, (cut - 1) * rows), (0, 128 - notes.shape[1])))
+    notes = jnp.pad(notes, ((0, 0), (0, 128 - notes.shape[1])))
+    out_parts = out_weight.shape[0] // rows
     payload = jnp.concatenate(
+        [normed_exact.astype(f16)]
+        + [out_weight[i * rows : (i + 1) * rows].astype(f16) for i in range(out_parts)]
+        + [notes],
+        axis=1,
+    )
+    payload, beside = lax.optimization_barrier((payload, beside))
+    column_weights = jnp.concatenate([own, beside], axis=0)
+    other_weights = from_peer(column_weights, "core")
+    gathered = lax.all_gather(payload, ROW, axis=0, tiled=True)
+    block_rows = gathered[:, :width].astype(bf16)
+    out_own = gathered[:, width : width * (1 + out_parts)]
+    out_beside = from_peer(out_own, "zb")
+    my_notes = gathered[:, width * (1 + out_parts) :].reshape(far, row // far, rows, 128)
+    at_mine = lax.dynamic_index_in_dim(
+        my_notes, lax.axis_index("zm"), axis=1, keepdims=False
+    ).astype(f32)
+
+    columns = jnp.concatenate(
         [
-            jnp.concatenate(
-                [normed_exact[:, i * piece : (i + 1) * piece] for i in range(cut)], axis=0
-            ).astype(f16),
-            jnp.concatenate([out_weight[:, :half], out_weight[:, half:]], axis=0).astype(f16),
-            shared_gate.astype(f16),
-            shared_up.astype(f16),
-            shared_down.T.astype(f16),
-            notes,
+            lax.dot_general(
+                block_rows, weights, (((1,), (1,)), ((), ())), preferred_element_type=f32
+            )
+            for weights in (column_weights, other_weights)
         ],
         axis=1,
-    )
-    gathered = lax.all_gather(payload, EP, axis=0, tiled=True)
-    whole = gathered[:, piece : piece + half + 3 * hidden]
-    chips_rows = gathered[:, :piece].reshape(ring, cores, cut, rows, piece)
-    chips_rows = lax.dynamic_index_in_dim(chips_rows, my_core, axis=1, keepdims=False)
-    block_rows = chips_rows.transpose(0, 2, 1, 3).reshape(ring * rows, width).astype(bf16)
-    my_notes = gathered[:, piece + half + 3 * hidden :].reshape(far, near, cut * rows, 128)
-    my_notes = lax.dynamic_index_in_dim(
-        my_notes[:, :, :rows], my_zb * cores + my_core, axis=1, keepdims=False
-    ).astype(f32)
-
-    pair = jnp.where(my_core == 0, jnp.stack([own, other]), jnp.stack([other, own]))
-    columns = lax.dot_general(
-        block_rows, pair.reshape(-1, width), (((1,), (1,)), ((), ())), preferred_element_type=f32
     ).astype(bf16)
     projected = lax.all_to_all(
-        columns.reshape(ring, rows, columns.shape[1]), RING, split_axis=0, concat_axis=0, tiled=True
-    )
-    share = query_weight.shape[1]
-    projected = projected.reshape(ring, rows, cores, 4, share).transpose(3, 1, 0, 2, 4)
+        columns.reshape(row, rows, columns.shape[1]), ROW, split_axis=0, concat_axis=0, tiled=True
+    )
+    projected, out_beside = lax.optimization_barrier((projected, out_beside))
+    out_pair = jnp.stack([out_own, out_beside])
+    out_other = from_peer(out_pair, "core")
+    projected = projected.reshape(row, rows, 2, 2, 4, share).transpose(4, 1, 0, 3, 2, 5)
+    projected = in_order(projected, ("zb", "core"), 3)
     projected = projected.reshape(4, rows, devices * share)
 
     slot_ids = jnp.arange(slots, dtype=f32)
-    at_mine = my_notes
     block_experts = (my_far * near).astype(f32) + jnp.arange(near, dtype=f32)
     hits = (at_mine[:, :, :top, None] == block_experts).astype(f32)
     weights = at_mine[:, :, top : 2 * top] + at_mine[:, :, 2 * top : 3 * top]
@@ -205,21 +211,50 @@
         max_state,
         head_gain,
     )
-    spread = gated.reshape(1, rows, devices, 1, -1) * jnp.eye(2, dtype=bf16).reshape(2, 1, 1, 2, 1)
-    mix_sums = jnp.dot(
-        spread.reshape(2 * rows, -1), whole[:, :half].astype(bf16), preferred_element_type=f32
-    )
-    mix_sums = jnp.concatenate([mix_sums[:rows], mix_sums[rows:]], axis=1)
+    spread = gated.reshape(rows, row, 2, 2, out_parts, -1).transpose(3, 2, 4, 0, 1, 5)
+    spread = in_order(spread, ("core", "zb"), 0).reshape(2, 2, out_parts, rows, -1)
+    mix_sums = jnp.zeros((rows, width), f32)
+    for core, halves in enumerate((out_pair, out_other)):
+        for zb in range(2):
+            for part in range(out_parts):
+                mix_sums = mix_sums + jnp.dot(
+                    spread[core, zb, part],
+                    halves[zb, :, part * width : (part + 1) * width].astype(bf16),
+                    preferred_element_type=f32,
+                )
     stream = inputs + mix_sums.astype(bf16).astype(f32)
-    normed_two = rounded(rms_scale(stream, second_gain), bf16).astype(bf16)
-
-    far_rows = lax.all_gather(normed_two, FAR, axis=0, tiled=True)
+    normed_exact = rounded(rms_scale(stream, second_gain), bf16)
+    normed_two = normed_exact.astype(bf16)
+
+    hidden = shared_gate.shape[1]
+    depth = shared_gate.shape[0]
+    cut = depth // rows
+    piece = width // cut
+    payload = jnp.concatenate(
+        [
+            jnp.concatenate(
+                [normed_exact[:, i * piece : (i + 1) * piece] for i in range(cut)], axis=0
+            ).astype(f16),
+            shared_gate.astype(f16),
+            shared_up.astype(f16),
+            shared_down.T.astype(f16),
+        ],
+        axis=1,
+    )
+    gathered = lax.all_gather(payload, FAR, axis=0, tiled=True)
+    far_rows = gathered[:, :piece].reshape(far, cut, rows, piece).transpose(0, 2, 1, 3)
+    far_rows = far_rows.reshape(far * rows, width).astype(bf16)
+    shared_one = gathered[:, piece:]
+    shared_beside = from_peer(shared_one, "zm")
     outgoing = lax.dot_general(
         selector, far_rows, (((0,), (0,)), ((), ())), preferred_element_type=f32
     ).astype(bf16)
     flat_rows = lax.all_to_all(
         outgoing.reshape(near, far * slots, width), NEAR, split_axis=0, concat_axis=0, tiled=True
     ).reshape(near * far * slots, width)
+    flat_rows, shared_beside = lax.optimization_barrier((flat_rows, shared_beside))
+    shared_two = jnp.stack([shared_one, shared_beside])
+    shared_beside = from_peer(shared_two, "zb")
     gate_sums = jnp.dot(flat_rows, expert_gate[0], preferred_element_type=f32)
     up_sums = jnp.dot(flat_rows, expert_up[0], preferred_element_type=f32)
     hidden_rows = (jax.nn.silu(gate_sums) * up_sums).astype(bf16)
@@ -227,6 +262,9 @@
     near_results = lax.all_to_all(
         result.reshape(near, far * slots, width), NEAR, split_axis=0, concat_axis=0, tiled=True
     ).reshape(near * far * slots, width)
+    near_results, shared_beside = lax.optimization_barrier((near_results, shared_beside))
+    shared_four = jnp.stack([shared_two, shared_beside])
+    shared_other = from_peer(shared_four, "core")
     partial = jnp.dot(mixer_high, near_results, preferred_element_type=f32) + jnp.dot(
         mixer_low, near_results, preferred_element_type=f32
     )
@@ -235,23 +273,34 @@
     )
     routed = jnp.sum(far_sums.astype(f32), axis=0)
 
-    gate_up = jnp.dot(
-        normed_two, whole[:, half : half + 2 * hidden].astype(bf16), preferred_element_type=f32
-    )
+    by_member = normed_two.reshape(rows, far, 2, 2, 2, depth).transpose(4, 3, 2, 0, 1, 5)
+    by_member = in_order(by_member, ("core", "zb", "zm"), 0).reshape(near, rows, far * depth)
+    shared_all = jnp.concatenate(
+        [shared_four.reshape(near // 2, far * depth, -1), shared_other.reshape(near // 2, far * depth, -1)]
+    ).astype(bf16)
+    gate_up = lax.dot_general(
+        by_member,
+        shared_all[:, :, : 2 * hidden],
+        (((2,), (1,)), ((0,), (0,))),
+        preferred_element_type=f32,
+    )
+    gate_up = jnp.sum(gate_up, axis=0)
     hidden_shared = (jax.nn.silu(gate_up[:, :hidden]) * gate_up[:, hidden:]).astype(bf16)
     shared_result = lax.dot_general(
         hidden_shared,
-        whole[:, half + 2 * hidden :].astype(bf16),
-        (((1,), (1,)), ((), ())),
+        shared_all[:, :, 2 * hidden :],
+        (((1,), (2,)), ((), ())),
         preferred_element_type=f32,
     )
+    shared_result = shared_result.reshape(rows, 2, 2, 2, far, depth).transpose(0, 4, 3, 2, 1, 5)
+    shared_result = in_order(shared_result, NEAR, 2).reshape(rows, width)
     mixed_out = (stream + routed + shared_result).astype(bf16)
     return (mixed_out, memory_next, norm_next, max_next)
 
 
 def solution(mesh):
     torus = Mesh(
-        mesh.devices.reshape(mesh.shape["grp"], 8, 4, 2), ("grp", "za", "zb", "core")
+        mesh.devices.reshape(mesh.shape["grp"], 8, 2, 2, 2), GRP_EP
     )
     placed = (
         P(GRP_EP, None),

time: 316 us -> 360 us (1.14)
  blocking collectives: 162 us -> 124 us
  waiting for transfers between devices: 73.6 us -> 110 us
  local copies, waits for them, and re-layouts: 11.8 us -> 31.9 us
  other arithmetic: 18.1 us -> 31.9 us
  starting transfers between devices: 30.1 us -> 36.7 us
  matrix products: 18 us -> 21.8 us
    ppermute x1 -> x7, waiting for transfers between devices: 0.01 us -> 51.6 us  [from_peer(): return lax.ppermute(values, axis, [(0, 1), (1, 0)])]
    all_gather x2, blocking collectives: 145 us -> 124 us  [the longest x1 79.3 us: shards(): gathered = lax.all_gather(payload, ROW, axis=0, tiled=True)]
    all_to_all x1 -> x0, blocking collectives: 16.9 us -> none  [shards(): lax.all_to_all(outgoing.reshape(near, far * slots, width), NEAR, split_ax...]
    all_to_all x1, waiting for transfers between devices: 11.7 us -> 0.01 us  [shards(): lax.all_to_all(result.reshape(near, far * slots, width), NEAR, split_axis...]
    convert_element_type x5 -> x10, other arithmetic: 1.35 us -> 8.28 us  [the longest x1 1.95 us: shards(): shared_all = jnp.concatenate([shared_four.reshape(near // 2, far * depth,...]
    unnamed x16 -> x40, local copies, waits for them, and re-layouts: 4.98 us -> 9.69 us
    reshape x0 -> x8, local copies, waits for them, and re-layouts: none -> 3.71 us  [the longest x2 2.55 us: shards(): projected.reshape(row, rows, 2, 2, 4, share).transpose(4, 1, 0, 3, 2, 5)]
    dot_general x5 -> x13, matrix products: 11 us -> 12.1 us  [the longest x8 5.77 us: shards(): jnp.dot(spread[core, zb, part], halves[zb, :, part * width:(part + 1) * w...]
  transfers between devices with their start and end apart: 4 -> 11, of which waited for: 3 -> 4; matrix products, arithmetic and copies ran while one was open for 5% -> 13% of each run, Pallas kernels for 0% -> 0%
where the time goes in v3:
time: 360 us; the launch traced here: 358 us
  blocking collectives  124 us (34%)
  waiting for transfers between devices  110 us (31%)
  starting transfers between devices  36.7 us (10%)
  local copies, waits for them, and re-layouts  31.9 us (9%)
  other arithmetic  31.9 us (9%)
  matrix products  21.8 us (6%)
    all_gather x1, blocking collectives, shards(): gathered = lax.all_gather(payload, ROW, axis=0, tiled=True)  79.3 us
    ppermute x7, waiting for transfers between devices, from_peer(): return lax.ppermute(values, axis, [(0, 1), (1, 0)])  51.6 us
    all_gather x1, blocking collectives, shards(): gathered = lax.all_gather(payload, FAR, axis=0, tiled=True)  45.1 us
    all_to_all x1, waiting for transfers between devices, shards(): lax.all_to_all(partial.astype(bf16).reshape(far, rows, width), FAR, split...  35.1 us
    all_to_all x1, waiting for transfers between devices, shards(): lax.all_to_all(columns.reshape(row, rows, columns.shape[1]), ROW, split_a...  23.3 us
    all_to_all x1, starting transfers between devices, shards(): lax.all_to_all(partial.astype(bf16).reshape(far, rows, width), FAR, split...  14.4 us
    unnamed x40, local copies, waits for them, and re-layouts  9.69 us
    all_to_all x1, starting transfers between devices, shards(): lax.all_to_all(columns.reshape(row, rows, columns.shape[1]), ROW, split_a...  8.88 us
  transfers between devices with their start and end apart: 11, of which 4 were waited for; matrix products, arithmetic and copies ran while one was open for 13% of the time, Pallas kernels for 0%

profile of v3, /device:TPU:102, one launch (start us, length us, event | category | flops | bytes accessed | tf_op | source)
XLA Modules:
  0.0 358.0 jit_solution(3707160827783618954)
XLA Ops:
  9.4 1.6 broadcast_multiply_fusion.1
  22.8 79.3 %all-gather.1 = f16[128,6272]{1,0:T(8,128)(2,1)S(1)} all-gather(f16[8,6272]{1,0:T(8,128)(2,1)S(1)} %pad_maximum_fusion.4), channel_id=1, replica_groups=mesh['grp'=4,'za'=8,'zm'=2,'zb'=2,'core'=2] {'za','zm'}, dimensions={0}, use_global_device_ids=true | all-gather | bytes 1705984 | tf_op jit(solution)/shard_map/all_gather | solution.py:156
  110.2 8.9 %all-to-all-start = ((bf16[16,8,256]{2,1,0:T(8,128)(2,1)}), bf16[16,8,256]{2,1,0:T(8,128)(2,1)S(1)}, u32[]{:S(2)}, u32[]{:S(2)}) async-start(bf16[16,8,256]{2,1,0:T(8,128)(2,1)} %pad_maximum_fusion.6), calls=%async_computation | async-start | bytes 131072 | tf_op jit(solution)/shard_map/all_to_all | solution.py:174
  120.2 23.3 %all-to-all-done = bf16[16,8,256]{2,1,0:T(8,128)(2,1)S(1)} async-done(((bf16[16,8,256]{2,1,0:T(8,128)(2,1)}), bf16[16,8,256]{2,1,0:T(8,128)(2,1)S(1)}, u32[]{:S(2)}, u32[]{:S(2)}) %all-to-all-start) | async-done | bytes 65568 | tf_op jit(solution)/shard_map/all_to_all | solution.py:174
  149.5 1.8 copy.62
  151.3 1.9 reshape.215
  155.4 1.8 copy.63
  157.1 1.9 reshape.216
  160.1 1.8 pad_maximum_fusion
  163.0 2.6 multiply_add_fusion
  165.6 2.0 fusion.82
  167.9 1.6 reshape.201
  177.9 45.1 %all_gather.7 = f16[256,1280]{1,0:T(8,128)(2,1)S(1)} all-gather(f16[32,1280]{1,0:T(8,128)(2,1)S(1)} %pad_maximum_fusion.5), channel_id=1, replica_groups=mesh['grp'=4,'za'=8,'zm'=2,'zb'=2,'core'=2] {'za'}, dimensions={0}, use_global_device_ids=true | all-gather | bytes 737280 | tf_op jit(solution)/shard_map/all_gather | solution.py:244
  224.1 3.6 all-to-all-start.1
  227.8 2.2 collective-permute-start.4
  230.0 26.1 %collective-permute-done.4 = f16[256,768]{1,0:T(8,128)(2,1)S(1)} collective-permute-done((f16[256,768]{1,0:T(8,128)(2,1)S(1)}, f16[256,768]{1,0:T(8,128)(2,1)S(1)}, u32[]{:S(2)}, u32[]{:S(2)}) %collective-permute-start.4) | collective-permute-done | bytes 393248 | tf_op jit(solution)/shard_map/ppermute | solution.py:77
  256.1 1.5 fusion.22
  257.6 2.8 convolution_convert_fusion
  260.5 7.0 %all-to-all-start.2 = ((bf16[8,16,2048]{2,1,0:T(8,128)(2,1)}), bf16[8,16,2048]{2,1,0:T(8,128)(2,1)S(1)}, u32[]{:S(2)}, u32[]{:S(2)}) async-start(bf16[8,16,2048]{2,1,0:T(8,128)(2,1)} %bitcast.47), calls=%async_computation.2 | async-start | bytes 1048576 | tf_op jit(solution)/shard_map/all_to_all | solution.py:262
  268.8 25.5 %collective-permute-done.5 = f16[2,256,768]{2,1,0:T(8,128)(2,1)S(1)} collective-permute-done((f16[2,256,768]{2,1,0:T(8,128)(2,1)S(1)}, f16[2,256,768]{2,1,0:T(8,128)(2,1)S(1)}, u32[]{:S(2)}, u32[]{:S(2)}) %collective-permute-start.5) | collective-permute-done | bytes 786464 | tf_op jit(solution)/shard_map/ppermute | solution.py:77
  295.2 1.7 pad_maximum_fusion.1
  301.6 14.4 %all-to-all-start.3 = ((bf16[8,8,2048]{2,1,0:T(8,128)(2,1)}), bf16[8,8,2048]{2,1,0:T(8,128)(2,1)S(1)}, u32[]{:S(2)}, u32[]{:S(2)}) async-start(bf16[8,8,2048]{2,1,0:T(8,128)(2,1)} %fusion.1), calls=%async_computation.3 | async-start | bytes 524288 | tf_op jit(solution)/shard_map/all_to_all | solution.py:271
  316.6 1.9 maximum_convert_fusion
  322.2 35.1 %all-to-all-done.3 = bf16[8,8,2048]{2,1,0:T(8,128)(2,1)S(1)} async-done(((bf16[8,8,2048]{2,1,0:T(8,128)(2,1)}), bf16[8,8,2048]{2,1,0:T(8,128)(2,1)S(1)}, u32[]{:S(2)}, u32[]{:S(2)}) %all-to-all-start.3) | async-done | bytes 262176 | tf_op jit(solution)/shard_map/all_to_all | solution.py:271
  (154 shorter events, 61.4 us)
Async XLA Ops:
  0.6 257.0 %copy-start = (bf16[1,256,2048]{2,1,0:T(8,128)(2,1)S(1)}, bf16[1,256,2048]{2,1,0:T(8,128)(2,1)}, u32[]{:S(2)}) copy-start(bf16[1,256,2048]{2,1,0:T(8,128)(2,1)} %param.44) | copy-start | bytes 3145732
  1.7 21.1 %collective-permute-start = (bf16[64,2048]{1,0:T(8,128)(2,1)S(1)}, bf16[64,2048]{1,0:T(8,128)(2,1)S(1)}, u32[]{:S(2)}, u32[]{:S(2)}) collective-permute-start(bf16[64,2048]{1,0:T(8,128)(2,1)S(1)} %pad_maximum_fusion.3), channel_id=1, source_target_pairs={{0,2},{2,0},{1,3},{3,1},{4,6},{6,4},{5,7},{7,5},{8,10},{10,8},{9,1... | collective-permute-start | bytes 786440 | tf_op jit(solution)/shard_map/ppermute | solution.py:77
  1.9 117.5 %copy-start.16 = (pred[8,8]{0,1:T(8,128)(4,1)}, pred[8,8]{0,1:T(8,128)(4,1)S(1)}, u32[]{:S(2)}) copy-start(pred[8,8]{0,1:T(8,128)(4,1)S(1)} %iota_compare_fusion.3) | copy-start | bytes 196
  105.2 2.8 collective-permute-start.1
  105.5 38.1 %collective-permute-start.2 = (f16[128,4096]{1,0:T(8,128)(2,1)}, f16[128,4096]{1,0:T(8,128)(2,1)S(1)}, u32[]{:S(2)}, u32[]{:S(2)}) collective-permute-start(f16[128,4096]{1,0:T(8,128)(2,1)} %get-tuple-element.28), channel_id=1, source_target_pairs={{0,2},{2,0},{1,3},{3,1},{4,6},{6,4},{5,7},{7,5},{8,10},{10,8},{9,1... | collective-permute-start | bytes 3145736 | tf_op jit(solution)/shard_map/ppermute | solution.py:77
  110.2 33.4 %all-to-all-start = ((bf16[16,8,256]{2,1,0:T(8,128)(2,1)}), bf16[16,8,256]{2,1,0:T(8,128)(2,1)S(1)}, u32[]{:S(2)}, u32[]{:S(2)}) async-start(bf16[16,8,256]{2,1,0:T(8,128)(2,1)} %pad_maximum_fusion.6), calls=%async_computation | async-start | bytes 131072 | tf_op jit(solution)/shard_map/all_to_all | solution.py:174
  159.0 2.9 copy-start.11
  159.0 2.9 copy-start.15
  160.1 2.9 copy-start.3
  161.9 10.8 %collective-permute-start.3 = (f16[2,128,4096]{2,1,0:T(8,128)(2,1)}, f16[2,128,4096]{2,1,0:T(8,128)(2,1)}, u32[]{:S(2)}, u32[]{:S(2)}) collective-permute-start(f16[2,128,4096]{2,1,0:T(8,128)(2,1)} %pad_maximum_fusion), channel_id=1, source_target_pairs={{0,1},{1,0},{2,3},{3,2},{4,5},{5,4},{6,7},{7,6},{8,9},{9,8},{10,11... | collective-permute-start | bytes 6291464 | tf_op jit(solution)/shard_map/ppermute | solution.py:77
  171.9 4.5 %copy-start.5 = (bf16[8,2048]{1,0:T(8,128)(2,1)S(1)}, bf16[8,2048]{1,0:T(8,128)(2,1)}, u32[]{:S(2)}) copy-start(bf16[8,2048]{1,0:T(8,128)(2,1)} %param.24) | copy-start | bytes 98308
  172.2 5.4 %copy-start.12 = (f32[2048]{0:T(1024)S(1)}, f32[2048]{0:T(1024)}, u32[]{:S(2)}) copy-start(f32[2048]{0:T(1024)} %convert_element_type.262) | copy-start | bytes 24580
  172.2 5.6 %copy-start.8 = (f16[32,256]{1,0:T(8,128)(2,1)S(1)}, f16[32,256]{1,0:T(8,128)(2,1)}, u32[]{:S(2)}) copy-start(f16[32,256]{1,0:T(8,128)(2,1)} %convert_element_type.263) | copy-start | bytes 49156
  172.2 5.6 %copy-start.9 = (f16[32,256]{1,0:T(8,128)(2,1)S(1)}, f16[32,256]{1,0:T(8,128)(2,1)}, u32[]{:S(2)}) copy-start(f16[32,256]{1,0:T(8,128)(2,1)} %convert_element_type.264) | copy-start | bytes 49156
  172.3 5.6 %copy-start.10 = (f16[32,256]{1,0:T(8,128)(2,1)S(1)}, f16[32,256]{1,0:T(8,128)(2,1)}, u32[]{:S(2)}) copy-start(f16[32,256]{1,0:T(8,128)(2,1)} %convert_bitcast_fusion) | copy-start | bytes 49156
  172.6 50.4 %copy-start.6 = (bf16[64,128]{0,1:T(8,128)(2,1)S(1)}, bf16[64,128]{0,1:T(8,128)(2,1)}, u32[]{:S(2)}) copy-start(bf16[64,128]{0,1:T(8,128)(2,1)} %convert_element_type.261) | copy-start | bytes 49156
  224.1 32.0 %all-to-all-start.1 = ((bf16[8,16,2048]{2,1,0:T(8,128)(2,1)}), bf16[8,16,2048]{2,1,0:T(8,128)(2,1)S(1)}, u32[]{:S(2)}, u32[]{:S(2)}) async-start(bf16[8,16,2048]{2,1,0:T(8,128)(2,1)} %bitcast.42), calls=%async_computation.1 | async-start | bytes 1048576 | tf_op jit(solution)/shard_map/all_to_all | solution.py:252
  227.8 28.3 %collective-permute-start.4 = (f16[256,768]{1,0:T(8,128)(2,1)S(1)}, f16[256,768]{1,0:T(8,128)(2,1)S(1)}, u32[]{:S(2)}, u32[]{:S(2)}) collective-permute-start(f16[256,768]{1,0:T(8,128)(2,1)S(1)} %get-tuple-element.32), channel_id=1, source_target_pairs={{0,4},{4,0},{1,5},{5,1},{2,6},{6,2},{3,7},{7,3},{8,12},{12,8},{9,1... | collective-permute-start | bytes 1179656 | tf_op jit(solution)/shard_map/ppermute | solution.py:77
  260.5 33.8 %all-to-all-start.2 = ((bf16[8,16,2048]{2,1,0:T(8,128)(2,1)}), bf16[8,16,2048]{2,1,0:T(8,128)(2,1)S(1)}, u32[]{:S(2)}, u32[]{:S(2)}) async-start(bf16[8,16,2048]{2,1,0:T(8,128)(2,1)} %bitcast.47), calls=%async_computation.2 | async-start | bytes 1048576 | tf_op jit(solution)/shard_map/all_to_all | solution.py:262
  268.5 28.6 %copy-start.17 = (pred[8,8]{0,1:T(8,128)(4,1)S(1)}, pred[8,8]{0,1:T(8,128)(4,1)}, u32[]{:S(2)}) copy-start(pred[8,8]{0,1:T(8,128)(4,1)} %copy-done.16) | copy-start | bytes 196
  268.5 28.8 %copy-start.7 = (f32[8,8,8]{2,1,0:T(8,128)S(1)}, f32[8,8,8]{2,1,0:T(8,128)}, u32[]{:S(2)}) copy-start(f32[8,8,8]{2,1,0:T(8,128)} %get-tuple-element.20) | copy-start | bytes 6148
  268.5 25.8 %collective-permute-start.5 = (f16[2,256,768]{2,1,0:T(8,128)(2,1)S(1)}, f16[2,256,768]{2,1,0:T(8,128)(2,1)S(1)}, u32[]{:S(2)}, u32[]{:S(2)}) collective-permute-start(f16[2,256,768]{2,1,0:T(8,128)(2,1)S(1)} %get-tuple-element.30), channel_id=1, source_target_pairs={{0,2},{2,0},{1,3},{3,1},{4,6},{6,4},{5,7},{7,5},{8,10},{10,8},{9,1... | collective-permute-start | bytes 2359304 | tf_op jit(solution)/shard_map/ppermute | solution.py:77
  297.0 19.7 %collective-permute-start.6 = (f16[2,2,256,768]{3,2,1,0:T(8,128)(2,1)S(1)}, f16[2,2,256,768]{3,2,1,0:T(8,128)(2,1)}, u32[]{:S(2)}, u32[]{:S(2)}) collective-permute-start(f16[2,2,256,768]{3,2,1,0:T(8,128)(2,1)S(1)} %pad_maximum_fusion.1), channel_id=1, source_target_pairs={{0,1},{1,0},{2,3},{3,2},{4,5},{5,4},{6,7},{7,6},{8,9},{9,8},{10,11... | collective-permute-start | bytes 4718600 | tf_op jit(solution)/shard_map/ppermute | solution.py:77
  301.6 55.7 %all-to-all-start.3 = ((bf16[8,8,2048]{2,1,0:T(8,128)(2,1)}), bf16[8,8,2048]{2,1,0:T(8,128)(2,1)S(1)}, u32[]{:S(2)}, u32[]{:S(2)}) async-start(bf16[8,8,2048]{2,1,0:T(8,128)(2,1)} %fusion.1), calls=%async_computation.3 | async-start | bytes 524288 | tf_op jit(solution)/shard_map/all_to_all | solution.py:271
  (5 other events, 6.9 us)
